TPU v7x, 256 devices: a whole 4x4x8 slice. The times are simulated.
256 devices in a mesh: sp: 32 (over z, x), tp: 8 (over y, core).
Axes of the slice: x: 4, y: 4, z: 8, core: 2. Of those that a mesh axis runs over, the one named last changes fastest.
Arguments:
- latents: bfloat16 [16384, 2048], P(('sp', 'tp')), may hold values from -6 to 6
- context: bfloat16 [512, 2048], P('sp'), may hold values from -6 to 6
- cond: float32 [2048], P('sp'), may hold values from -6 to 6
- ctx_cond: float32 [2048], P('sp'), may hold values from -6 to 6
- mod_weight: float32 [2048, 6144], P('sp', 'tp'), may hold values from -0.125 to 0.125
- query_weight: bfloat16 [2048, 2048], P(None, 'tp'), may hold values from -1 to 1, as said below
- key_matrix: bfloat16 [2048, 1024], P(None, 'tp'), may hold values from -1 to 1, as said below
- value_matrix: bfloat16 [2048, 1024], P(None, 'tp'), may hold values from -0.125 to 0.125
- out_weight: bfloat16 [2048, 2048], P('tp'), may hold values from -0.125 to 0.125
- query_gain: float32 [128], replicated, may hold values from 0.7 to 7
- key_gain: float32 [128], replicated, may hold values from 0.7 to 7
Outputs:
- updated: bfloat16 [16384, 2048], P(('sp', 'tp'))
Inputs may be any that keep to these rules, and one draw needn't show every extreme that they name: `query_weight`: entries of order 2048 to the power -1/2. `key_matrix`: entries of order 2048 to the power -1/2.
All inputs are finite; a program needn't handle non-finite values.
Results may differ from a plain program's by a relative error of at most 0.0085.
The roundings to bfloat16 on the way count: a program that leaves them out, or rounds other values in their place, can miss the bound.
Values may be sent and summed in bfloat16 or wider, within the bound.
A program may use at most 128 MiB of HBM per device.

v0:
```python
import math

import jax
import jax.numpy as jnp
from jax import lax
from jax.sharding import Mesh
from jax.sharding import PartitionSpec as P

GRID_W = 64
SP = ("sp_0", "sp_1")
SP_TP = ("sp_0", "sp_1", "tp")


NORM_EPS = 1e-06
ROPE_BASE = 10000.0


def over_axes(value, axes):
    for axis in axes:
        value = lax.psum(value, axis)
    return value


def side_by_side(arrays, axis, dim, along):
    both = jnp.concatenate(arrays, axis=along)
    filled, at, done = (lax.all_gather(both, axis, axis=dim, tiled=True), 0, [])
    for a in arrays:
        done.append(lax.slice_in_dim(filled, at, at + a.shape[along], axis=along))
        at += a.shape[along]
    return tuple(done)


def normalize(latent_value_rows):
    return latent_value_rows * lax.rsqrt(
        jnp.mean(latent_value_rows * latent_value_rows, axis=-1, keepdims=True) + NORM_EPS
    )


def rotate(latent_value_rows, positions):
    quarter = latent_value_rows.shape[-1] // 2
    inv_freq = ROPE_BASE ** (-jnp.arange(quarter, dtype=jnp.float32) / quarter)
    angles = positions.astype(jnp.float32)[:, None] * inv_freq[None, :]
    cos_table = jnp.cos(angles)[:, None, :]
    sin_table = jnp.sin(angles)[:, None, :]
    first, second = (latent_value_rows[..., :quarter], latent_value_rows[..., quarter:])
    return jnp.concatenate(
        [first * cos_table - second * sin_table, second * cos_table + first * sin_table], axis=-1
    )


def axial(latent_value_rows, positions):
    half_dim = latent_value_rows.shape[-1] // 2
    return jnp.concatenate(
        [
            rotate(latent_value_rows[..., :half_dim], positions // GRID_W),
            rotate(latent_value_rows[..., half_dim:], positions % GRID_W),
        ],
        axis=-1,
    )


def modulate(latent_value_rows, mod_row):
    model_width = latent_value_rows.shape[-1]
    shift_vec = mod_row[:model_width]
    scale_vec = mod_row[model_width : 2 * model_width]
    return (
        normalize(latent_value_rows.astype(jnp.float32)) * (1.0 + scale_vec) + shift_vec
    ).astype(jnp.bfloat16)


def body(
    latents,
    context,
    cond,
    ctx_cond,
    mod_weight,
    query_weight,
    key_matrix,
    value_matrix,
    out_weight,
    query_gain,
    key_gain,
):
    model_width = latents.shape[1]
    head_dim = query_gain.shape[0]
    sp_count = lax.axis_size(SP)
    partials = jnp.dot(
        jax.nn.silu(jnp.stack([cond, ctx_cond])), mod_weight, precision=lax.Precision.HIGHEST
    )
    summed = over_axes(partials, SP)
    modulation = lax.all_gather(summed, "tp", axis=1, tiled=True)
    gate_vec = modulation[0, 2 * model_width :]
    normalised_rows = modulate(latents, modulation[0])
    prefix_normalised = modulate(context, modulation[1])
    query_cols = query_weight.shape[1]
    key_cols = key_matrix.shape[1]
    piece = lax.all_gather(normalised_rows, "tp", axis=0, tiled=True)
    projected = jnp.concatenate(
        [
            jnp.dot(piece, query_weight, preferred_element_type=jnp.float32),
            jnp.dot(piece, key_matrix, preferred_element_type=jnp.float32),
            jnp.dot(piece, value_matrix, preferred_element_type=jnp.float32),
        ],
        axis=1,
    )
    row_count = projected.shape[0]
    positions = lax.axis_index(SP) * row_count + jnp.arange(row_count, dtype=jnp.int32)
    query_heads = projected[:, :query_cols].reshape(row_count, -1, head_dim)
    query_heads = axial(normalize(query_heads) * query_gain, positions).astype(jnp.bfloat16)
    key_heads = projected[:, query_cols : query_cols + key_cols].reshape(row_count, -1, head_dim)
    key_heads = axial(normalize(key_heads) * key_gain, positions).astype(jnp.bfloat16)
    value_heads = (
        projected[:, query_cols + key_cols :].reshape(row_count, -1, head_dim).astype(jnp.bfloat16)
    )
    key_part = jnp.dot(prefix_normalised, key_matrix, preferred_element_type=jnp.float32).reshape(
        prefix_normalised.shape[0], -1, head_dim
    )
    value_part = jnp.dot(
        prefix_normalised, value_matrix, preferred_element_type=jnp.float32
    ).reshape(prefix_normalised.shape[0], -1, head_dim)
    local_keys = (normalize(key_part) * key_gain).astype(jnp.bfloat16)
    local_values = value_part.astype(jnp.bfloat16)
    prefix_keys, prefix_values = side_by_side((local_keys, local_values), SP, 0, 1)
    kv_local = key_heads.shape[1]
    group_size = query_heads.shape[1] // kv_local
    grouped = query_heads.reshape(row_count, kv_local, group_size, head_dim).transpose(1, 2, 0, 3)
    grouped = grouped.reshape(kv_local, group_size * row_count, head_dim)
    inv_root = head_dim ** (-0.5)
    lift = math.log(sp_count * row_count / (2.0 * prefix_keys.shape[0]))
    ctx_scores = (
        jnp.einsum("hqd,khd->hqk", grouped, prefix_keys, preferred_element_type=jnp.float32)
        * inv_root
        + lift
    )
    top_init = jnp.max(ctx_scores, axis=-1)
    ctx_weights = jnp.exp(ctx_scores - top_init[..., None])
    initial = (
        top_init,
        jnp.sum(ctx_weights, axis=-1),
        jnp.einsum(
            "hqk,khd->hqd",
            ctx_weights.astype(jnp.bfloat16),
            prefix_values,
            preferred_element_type=jnp.float32,
        ),
    )

    def update(state_now, key_block, value_block):
        top_old, total_old, acc_old = state_now
        scores = (
            jnp.einsum("hqd,khd->hqk", grouped, key_block, preferred_element_type=jnp.float32)
            * inv_root
        )
        top_new = jnp.maximum(top_old, jnp.max(scores, axis=-1))
        factor = jnp.exp(top_old - top_new)
        weights_now = jnp.exp(scores - top_new[..., None])
        acc_new = acc_old * factor[..., None] + jnp.einsum(
            "hqk,khd->hqd",
            weights_now.astype(jnp.bfloat16),
            value_block,
            preferred_element_type=jnp.float32,
        )
        return (top_new, total_old * factor + jnp.sum(weights_now, axis=-1), acc_new)

    key_piece, value_piece = side_by_side((key_heads, value_heads), SP, 0, 1)
    key_count = key_piece.shape[0]
    rows_per_block = math.gcd(key_count, 2048)
    block_count = key_count // rows_per_block
    key_blocks = key_piece.reshape(block_count, rows_per_block, kv_local, head_dim)
    value_blocks = value_piece.reshape(block_count, rows_per_block, kv_local, head_dim)

    def one_step(state_in, blocks_in):
        return (update(state_in, blocks_in[0], blocks_in[1]), None)

    state_out, _ = lax.scan(one_step, initial, (key_blocks, value_blocks))
    top_fin, total_fin, acc_fin = state_out
    attended = (acc_fin / total_fin[..., None]).astype(jnp.bfloat16)
    attended = (
        attended.reshape(kv_local, group_size, row_count, head_dim)
        .transpose(2, 0, 1, 3)
        .reshape(row_count, -1)
    )
    exchanged = lax.all_to_all(attended, "tp", split_axis=0, concat_axis=1, tiled=True)
    mixed_rows = jnp.dot(
        exchanged,
        lax.all_gather(out_weight, "tp", axis=0, tiled=True),
        preferred_element_type=jnp.float32,
    )
    return (latents.astype(jnp.float32) + gate_vec * normalize(mixed_rows)).astype(jnp.bfloat16)


def solution(mesh):
    torus = Mesh(mesh.devices.reshape(8, 4, mesh.shape["tp"]), ("sp_0", "sp_1", "tp"))
    placed = (
        P(SP_TP, None),
        P(SP, None),
        P(SP),
        P(SP),
        P(SP, "tp"),
        P(None, "tp"),
        P(None, "tp"),
        P(None, "tp"),
        P("tp", None),
        P(),
        P(),
    )
    return jax.shard_map(
        body, mesh=torus, in_specs=placed, out_specs=P(SP_TP, None), check_vma=False
    )
```

profile of v0, /device:TPU:1, one launch (start us, length us, event | category | flops | bytes accessed | tf_op | source)
XLA Modules:
  0.0 285.0 jit_solution(6609689054624795851)
XLA Ops:
  7.8 17.5 %psum.14 = f32[2,768]{1,0:T(2,128)S(1)} all-reduce(f32[2,768]{1,0:T(2,128)S(1)} %fusion.67), channel_id=1, replica_groups=mesh['sp_0'=8,'sp_1'=4,'tp'=8] {'sp_0'}, use_global_device_ids=true, to_apply=%region_0.1 | all-reduce | flops 1536 | bytes 12288 | tf_op jit(solution)/shard_map/psum | solution.py:20
  25.3 8.6 %psum.15 = f32[2,768]{1,0:T(2,128)S(1)} all-reduce(f32[2,768]{1,0:T(2,128)S(1)} %psum.14), channel_id=1, replica_groups=mesh['sp_0'=8,'sp_1'=4,'tp'=8] {'sp_1'}, use_global_device_ids=true, to_apply=%region_1.2 | all-reduce | flops 1536 | bytes 12288 | tf_op jit(solution)/shard_map/psum | solution.py:20
  33.9 19.5 %all_gather.15 = f32[2,6144]{1,0:T(2,128)S(1)} all-gather(f32[2,768]{1,0:T(2,128)S(1)} %psum.15), channel_id=1, replica_groups=mesh['sp_0'=8,'sp_1'=4,'tp'=8] {'tp'}, dimensions={1}, use_global_device_ids=true | all-gather | bytes 55296 | tf_op jit(solution)/shard_map/all_gather | solution.py:91
  56.5 23.1 %all-gather.4.cloned.1.call-done = bf16[512,2048]{1,0:T(8,128)(2,1)} async-done(((bf16[64,2048]{1,0:T(8,128)(2,1)}), bf16[512,2048]{1,0:T(8,128)(2,1)}) %all-gather.4.cloned.1.call-update) | async-done | bytes 2097168 | tf_op jit(solution)/shard_map/all_gather | solution.py:97
  79.5 2.5 multiply_reduce_fusion.3
  82.7 2.5 fusion.22
  86.8 3.0 %multiply_cosine_fusion.1 = (f32[512,32]{1,0:T(8,128)S(1)}, f32[512,32]{1,0:T(8,128)}, f32[512,32]{1,0:T(8,128)}, f32[512,32]{1,0:T(8,128)}) fusion(f32[32]{0:T(128)S(1)} %multiply_power_fusion, f32[512]{0:T(512)S(1)} %get-tuple-element.112, f32[512]{0:T(512)S(1)} %get-tuple-element.113), kind=kLoop, calls=%fused_computation.50 | loop fusion | flops 32768 | bytes 266368 | tf_op jit(solution)/shard_map/cos | solution.py:43
  92.6 40.4 %all_gather.17 = bf16[512,2,128]{2,0,1:T(8,128)(2,1)} all-gather(bf16[16,2,128]{2,0,1:T(8,128)(2,1)S(1)} %pad_maximum_fusion.2), channel_id=1, replica_groups=mesh['sp_0'=8,'sp_1'=4,'tp'=8] {'sp_0','sp_1'}, dimensions={0}, use_global_device_ids=true | all-gather | bytes 270336 | tf_op jit(solution)/shard_map/all_gather | solution.py:26
  139.6 46.4 %all-gather.6.cloned.1.call-done = bf16[16384,2,128]{0,2,1:T(8,128)(2,1)} async-done(((bf16[512,2,128]{0,2,1:T(8,128)(2,1)}), bf16[16384,2,128]{0,2,1:T(8,128)(2,1)}) %all-gather.6.cloned.1.call-update) | async-done | bytes 8388624 | tf_op jit(solution)/shard_map/all_gather | solution.py:26
  186.1 5.8 %fusion.76 = (bf16[16384,1,128]{0,2,1:T(8,128)(2,1)}, bf16[16384,1,128]{0,2,1:T(8,128)(2,1)}) fusion(bf16[16384,2,128]{0,2,1:T(8,128)(2,1)} %all-gather.6.cloned.1.call-done), kind=kLoop, calls=%fused_computation.126 | loop fusion | bytes 16777216 | tf_op jit(solution)/shard_map/slice | solution.py:28
  191.9 6.3 %copy.23 = bf16[16384,1,128]{2,0,1:T(8,128)(2,1)} copy(bf16[16384,1,128]{0,2,1:T(8,128)(2,1)} %get-tuple-element.78) | data formatting | bytes 8388608 | tf_op jit(solution)/shard_map/while | solution.py:175
  198.2 6.5 %copy.24 = bf16[16384,1,128]{2,0,1:T(8,128)(2,1)} copy(bf16[16384,1,128]{0,2,1:T(8,128)(2,1)} %get-tuple-element.77) | data formatting | bytes 8388608 | tf_op jit(solution)/shard_map/while | solution.py:175
  204.7 52.6 %while.14 = (s32[]{:T(128)}, f32[1,1024]{1,0:T(1,128)S(1)}, f32[1,1024]{1,0:T(1,128)S(1)}, f32[1,1024,128]{2,1,0:T(8,128)S(1)}, bf16[8,2048,1,128]{3,1,2,0:T(8,1...) while((s32[]{:T(128)}, f32[1,1024]{1,0:T(1,128)S(1)}, ...), condition=%wide.region_12.13_spmd, body=%wide.region_9.12_spmd.sunk | while | flops 1090783232 | bytes 27590756 | solution.py:175
  204.7 2.3 multiply_reduce_fusion.6
  208.5 2.8 fusion.97
  215.1 2.8 fusion.97
  221.6 2.8 fusion.97
  228.2 2.8 fusion.97
  234.8 2.8 fusion.97
  241.4 2.8 fusion.97
  247.9 2.8 fusion.97
  254.5 2.8 fusion.97
  258.0 14.5 %all_to_all.19 = bf16[8,64,256]{2,1,0:T(8,128)(2,1)S(1)} all-to-all(bf16[8,64,256]{2,1,0:T(8,128)(2,1)S(1)} %all_to_all.14), channel_id=1, replica_groups=mesh['sp_0'=8,'sp_1'=4,'tp'=8] {'tp'}, dimensions={0} | all-to-all | bytes 524288 | tf_op jit(solution)/shard_map/all_to_all | solution.py:183
  272.5 5.1 %multiply_reduce_fusion.1 = (f32[64]{0:T(128)S(1)}, f32[64,2048]{1,0:T(8,128)S(1)}) fusion(bf16[64,2048]{1,0:T(8,128)(2,1)S(1)} %bitcast.110, bf16[2048,2048]{1,0:T(8,128)(2,1)} %all-gather.8.cloned.1.call-done), kind=kOutput, calls=%fused_computation.39 | convolution fusion | flops 537132992 | bytes 9175296 | tf_op jit(solution)/shard_map/dot_general | solution.py:184
  (93 shorter events, 45.2 us)
Async XLA Ops:
  6.5 126.6 %copy-start = (bf16[2048,256]{1,0:T(8,128)(2,1)S(1)}, bf16[2048,256]{1,0:T(8,128)(2,1)}, u32[]{:S(2)}) copy-start(bf16[2048,256]{1,0:T(8,128)(2,1)} %param.18) | copy-start | bytes 3145732
  6.5 75.5 %copy-start.5 = (f32[128]{0:T(128)S(1)}, f32[128]{0:T(128)}, u32[]{:S(2)}) copy-start(f32[128]{0:T(128)} %param.23) | copy-start | bytes 1540
  6.5 73.0 %all-gather.4.cloned.1.call-start = ((), (), s32[]{:S(2)}) async-start(), calls=%async_computation.1 | async-start | bytes 2359296 | tf_op jit(solution)/shard_map/all_gather | solution.py:97
  56.4 129.7 %all-gather.6.cloned.1.call-start = ((), (), s32[]{:S(2)}) async-start(), calls=%async_computation.2 | async-start | bytes 8650752 | tf_op jit(solution)/shard_map/all_gather | solution.py:26
  56.4 33.3 %copy-start.4 = (bf16[16,2048]{1,0:T(8,128)(2,1)S(1)}, bf16[16,2048]{1,0:T(8,128)(2,1)}, u32[]{:S(2)}) copy-start(bf16[16,2048]{1,0:T(8,128)(2,1)} %param.14) | copy-start | bytes 196612
  82.1 51.0 %copy-start.1 = (bf16[512,2048]{1,0:T(8,128)(2,1)S(1)}, bf16[512,2048]{1,0:T(8,128)(2,1)}, u32[]{:S(2)}) copy-start(bf16[512,2048]{1,0:T(8,128)(2,1)} %all-gather.4.cloned.1.call-done) | copy-start | bytes 6291460
  86.0 49.9 %copy-start.6 = (f32[128]{0:T(128)S(1)}, f32[128]{0:T(128)}, u32[]{:S(2)}) copy-start(f32[128]{0:T(128)} %param.22) | copy-start | bytes 1540
  86.0 186.5 %all-gather.8.cloned.1.call-start = ((), (), s32[]{:S(2)}) async-start(), calls=%async_computation.3 | async-start | bytes 9437184 | tf_op jit(solution)/shard_map/all_gather | solution.py:186
  134.7 3.5 %copy-start.3 = (bf16[512,2,128]{2,0,1:T(8,128)(2,1)S(1)}, bf16[512,2,128]{2,0,1:T(8,128)(2,1)}, u32[]{:S(2)}) copy-start(bf16[512,2,128]{2,0,1:T(8,128)(2,1)} %all_gather.17) | copy-start | bytes 786436
  272.5 5.1 %copy-start.2 = (bf16[64,2048]{1,0:T(8,128)(2,1)S(1)}, bf16[64,2048]{1,0:T(8,128)(2,1)}, u32[]{:S(2)}) copy-start(bf16[64,2048]{1,0:T(8,128)(2,1)} %param.13) | copy-start | bytes 786436
Sparse Core Ops, SparseCore 0:
  56.5 23.0 all-gather.3
  86.1 99.8 all-gather.5
  187.9 54.6 all-gather.7
where the time goes:
time: 286 us; the launch traced here: 285 us
  blocking collectives  100 us (35%)
  waiting for transfers between devices  70.3 us (25%)
  matrix products  57.2 us (20%)
  other arithmetic  22.9 us (8%)
  local copies, waits for them, and re-layouts  20.4 us (7%)
  between operations  13.4 us (5%)
    all_gather x1, waiting for transfers between devices, side_by_side(): filled, at, done = (lax.all_gather(both, axis, axis=dim, tiled=True), 0, [])  46.4 us
    all_gather x1, blocking collectives, side_by_side(): filled, at, done = (lax.all_gather(both, axis, axis=dim, tiled=True), 0, [])  40.4 us
    psum x2, blocking collectives, over_axes(): value = lax.psum(value, axis)  26.1 us
    all_gather x1, waiting for transfers between devices, body(): piece = lax.all_gather(normalised_rows, 'tp', axis=0, tiled=True)  23.1 us
    dot_general x8, matrix products, update(): jnp.einsum('hqk,khd->hqd', weights_now.astype(jnp.bfloat16), value_block,...  22.2 us
    all_gather x1, blocking collectives, body(): modulation = lax.all_gather(summed, 'tp', axis=1, tiled=True)  19.5 us
    dot_general x8, matrix products, update(): jnp.einsum('hqd,khd->hqk', grouped, key_block, preferred_element_type=jnp...  18.4 us
    all_to_all x1, blocking collectives, body(): lax.all_to_all(attended, 'tp', split_axis=0, concat_axis=1, tiled=True)  14.5 us
  transfers between devices with their start and end apart: 3, of which 2 were waited for; matrix products, arithmetic and copies ran while one was open for 29% of the time, Pallas kernels for 0%

commit v1 on v0

v1 whole, which is shorter than its diff:
```python
import functools
import math

import jax
import jax.numpy as jnp
import numpy as np
from jax import lax
from jax.experimental import pallas as pl
from jax.experimental.pallas import tpu as pltpu
from jax.sharding import Mesh
from jax.sharding import PartitionSpec as P

MESH_ID = pl.DeviceIdType.MESH
GRID_W = 64
NORM_EPS = 1e-06
ROPE_BASE = 10000.0
NZ, NX, NY, NC = 8, 4, 4, 2
NTP = NY * NC
BF16, F32 = jnp.bfloat16, jnp.float32
VMEM_SPEC = pl.BlockSpec(memory_space=pltpu.VMEM)


def remote(src, dst, send_sem, recv_sem, **to):
    return pltpu.make_async_remote_copy(
        src_ref=src,
        dst_ref=dst,
        send_sem=send_sem,
        recv_sem=recv_sem,
        device_id=to,
        device_id_type=MESH_ID,
    )


def greet(peers):
    barrier = pltpu.get_barrier_semaphore()
    for peer in peers:
        pl.semaphore_signal(barrier, inc=1, device_id=peer, device_id_type=MESH_ID)
    pl.semaphore_wait(barrier, len(peers))


def tp_peers(y, c):
    peers = [{"c": 1 - c}]
    for dy in range(1, NY):
        for dc in range(NC):
            peers.append({"y": lax.rem(y + dy, NY), "c": lax.rem(c + dc, NC)})
    return peers


def tp_index(peer, y, c):
    return peer.get("y", y) * NC + peer["c"]


def diagonal(n):
    return lax.broadcasted_iota(jnp.int32, (n, n), 0) == lax.broadcasted_iota(jnp.int32, (n, n), 1)


def gather_kernel(
    lat, cond, ctx_cond, mod_weight, rows, mod, part, px, pt, zbuf, xbuf, tbuf, rs, rr, zs, zr, xs, xr, ts, tr
):
    z, x, y, c = (lax.axis_index(a) for a in ("z", "x", "y", "c"))
    me = y * NC + c
    yp, ym = lax.rem(y + 1, NY), lax.rem(y + NY - 1, NY)
    n = lat.shape[0]
    half = n // 2
    z_to = [{"z": lax.rem(z + d, NZ)} for d in range(1, NZ)]
    x_to = [{"x": lax.rem(x + d, NX)} for d in range(1, NX)]
    t_to = tp_peers(y, c)
    greet(z_to + x_to + t_to)

    up = remote(lat, rows.at[me], rs.at[0], rr.at[0], y=yp)
    down = remote(lat, rows.at[me], rs.at[1], rr.at[1], y=ym)
    over = remote(lat, rows.at[me], rs.at[2], rr.at[2], c=1 - c)
    up.start()
    down.start()
    over.start()

    eye = diagonal(cond.shape[1])
    for r, ref in enumerate((cond, ctx_cond)):
        v = ref[...]
        v = v * jax.nn.sigmoid(v)
        column = jnp.sum(jnp.where(eye, jnp.broadcast_to(v, eye.shape), 0.0), axis=1, keepdims=True)
        part[r : r + 1, :] = jnp.sum(column * mod_weight[...], axis=0, keepdims=True)
    z_out = [remote(part, zbuf.at[z], zs.at[i], zr.at[i], **to) for i, to in enumerate(z_to)]
    for cp in z_out:
        cp.start()
    zbuf[z] = part[...]
    rows[me] = lat[...]
    for cp in z_out:
        cp.wait_recv()
    px[...] = sum((zbuf[i] for i in range(1, NZ)), zbuf[0])
    x_out = [remote(px, xbuf.at[x], xs.at[i], xr.at[i], **to) for i, to in enumerate(x_to)]
    for cp in x_out:
        cp.start()
    xbuf[x] = px[...]

    up.wait_recv()
    down.wait_recv()
    low, high = ym * NC + c, yp * NC + c
    far = lax.rem(y + 2, NY) * NC + c
    up2 = remote(rows.at[low, 0:half], rows.at[low, 0:half], rs.at[3], rr.at[3], y=yp)
    down2 = remote(rows.at[high, half:n], rows.at[high, half:n], rs.at[4], rr.at[4], y=ym)
    up2.start()
    down2.start()
    over1 = remote(rows.at[low], rows.at[low], rs.at[5], rr.at[5], c=1 - c)
    over2 = remote(rows.at[high], rows.at[high], rs.at[6], rr.at[6], c=1 - c)
    over1.start()
    over2.start()

    for cp in x_out:
        cp.wait_recv()
    pt[...] = sum((xbuf[i] for i in range(1, NX)), xbuf[0])
    t_out = [remote(pt, tbuf.at[me], ts.at[i], tr.at[i], **to) for i, to in enumerate(t_to)]
    for cp in t_out:
        cp.start()
    tbuf[me] = pt[...]

    up2.wait_recv()
    down2.wait_recv()
    over3 = remote(rows.at[far], rows.at[far], rs.at[7], rr.at[7], c=1 - c)
    over3.start()
    for cp in t_out:
        cp.wait_recv()
    w = part.shape[1]
    for i in range(NTP):
        mod[:, i * w : (i + 1) * w] = tbuf[i]
    for cp in (over, over1, over2, over3):
        cp.wait_recv()
    for cp in [up, down, over, up2, down2, over1, over2, over3] + z_out + x_out + t_out:
        cp.wait_send()


def gather_stage(latents, cond, ctx_cond, mod_weight):
    n, d = latents.shape
    cols = mod_weight.shape[1]
    dma = pltpu.SemaphoreType.DMA
    return pl.pallas_call(
        gather_kernel,
        name="gather_stage",
        out_shape=(
            jax.ShapeDtypeStruct((NTP, n, d), BF16),
            jax.ShapeDtypeStruct((2, NTP * cols), F32),
        ),
        in_specs=[VMEM_SPEC] * 4,
        out_specs=(VMEM_SPEC, VMEM_SPEC),
        scratch_shapes=[
            pltpu.VMEM((2, cols), F32),
            pltpu.VMEM((2, cols), F32),
            pltpu.VMEM((2, cols), F32),
            pltpu.VMEM((NZ, 2, cols), F32),
            pltpu.VMEM((NX, 2, cols), F32),
            pltpu.VMEM((NTP, 2, cols), F32),
            dma((8,)),
            dma((8,)),
            dma((NZ - 1,)),
            dma((NZ - 1,)),
            dma((NX - 1,)),
            dma((NX - 1,)),
            dma((NTP - 1,)),
            dma((NTP - 1,)),
        ],
        compiler_params=pltpu.CompilerParams(collective_id=0, has_side_effects=True),
    )(latents, cond[None, :], ctx_cond[None, :], mod_weight)


def rope_tables(row_tokens, freqs):
    c = freqs // 4
    inv = (ROPE_BASE ** (-np.arange(c, dtype=np.float32) / np.float32(c))).astype(np.float32)

    def table(count, lanes_from):
        angles = np.arange(count, dtype=np.float32)[:, None] * inv[None, :]
        cos, sin = np.cos(angles), np.sin(angles)
        out_c = np.zeros((count, freqs), np.float32)
        out_s = np.zeros((count, freqs), np.float32)
        out_c[:, lanes_from : lanes_from + 2 * c] = np.concatenate([cos, cos], 1)
        out_s[:, lanes_from : lanes_from + 2 * c] = np.concatenate([-sin, sin], 1)
        return out_c, out_s

    return table(row_tokens, 0) + table(GRID_W, freqs // 2)


def rms(v):
    return v * lax.rsqrt(jnp.mean(v * v, axis=-1, keepdims=True) + NORM_EPS)


def project_kernel(rows, ctx, mod, wq, wk, wv, qg, kg, row_c, row_s, col_c, col_s, q_out, kv_out):
    step = pl.program_id(0)
    d = wq.shape[0]
    hd = wk.shape[1]
    count = rows.shape[0] * rows.shape[1]
    n_ctx = ctx.shape[0]
    sp = lax.axis_index("z") * NX + lax.axis_index("x")
    groups = count // GRID_W

    def modulated(v, r):
        v = rms(v.astype(F32))
        return (v * (1.0 + mod[r : r + 1, d : 2 * d]) + mod[r : r + 1, 0:d]).astype(BF16)

    steps = pl.num_programs(0)
    first = (sp * steps + step) * groups
    cos = jnp.concatenate([row_c[pl.ds(first + g, 1), :] + col_c[...] for g in range(groups)], axis=0)
    sin = jnp.concatenate([row_s[pl.ds(first + g, 1), :] + col_s[...] for g in range(groups)], axis=0)
    lane = lax.broadcasted_iota(jnp.int32, (count, hd), 1)
    early = lax.rem(lane, hd // 2) < hd // 4

    def turned(v):
        other = jnp.where(early, pltpu.roll(v, hd - hd // 4, 1), pltpu.roll(v, hd // 4, 1))
        return v * cos + other * sin

    a = modulated(rows[...].reshape(count, d), 0)
    q = jnp.dot(a, wq[...], preferred_element_type=F32)
    k = jnp.dot(a, wk[...], preferred_element_type=F32)
    v = jnp.dot(a, wv[...], preferred_element_type=F32)
    at = pl.multiple_of(step * count, count)
    for h in range(q_out.shape[0]):
        q_out[h, pl.ds(at, count), :] = turned(rms(q[:, h * hd : (h + 1) * hd]) * qg[...]).astype(BF16)
    kv_out[pl.ds(at, count), 0:hd] = turned(rms(k) * kg[...]).astype(BF16)
    kv_out[pl.ds(at, count), hd : 2 * hd] = v.astype(BF16)

    @pl.when(step == 0)
    def _():
        b = modulated(ctx[...], 1)
        kc = jnp.dot(b, wk[...], preferred_element_type=F32)
        vc = jnp.dot(b, wv[...], preferred_element_type=F32)
        end = kv_out.shape[0]
        kv_out[end - n_ctx : end, 0:hd] = (rms(kc) * kg[...]).astype(BF16)
        kv_out[end - n_ctx : end, hd : 2 * hd] = vc.astype(BF16)


def project_stage(rows, ctx, mod, wq, wk, wv, qg, kg):
    ntp, n, d = rows.shape
    hd = qg.shape[0]
    heads = wq.shape[1] // hd
    total = ntp * n
    steps = 2
    tables = rope_tables(NZ * NX * total // GRID_W, hd)
    whole = lambda a: pl.BlockSpec(a.shape, lambda i: (0,) * a.ndim)
    rest = (ctx, mod, wq, wk, wv, qg[None, :], kg[None, :]) + tuple(jnp.asarray(t) for t in tables)
    kv_rows = total + ctx.shape[0]
    return pl.pallas_call(
        project_kernel,
        name="project_stage",
        grid=(steps,),
        out_shape=(
            jax.ShapeDtypeStruct((heads, total, hd), BF16),
            jax.ShapeDtypeStruct((kv_rows, 2 * hd), BF16),
        ),
        in_specs=[pl.BlockSpec((ntp // steps, n, d), lambda i: (i, 0, 0))] + [whole(a) for a in rest],
        out_specs=(
            pl.BlockSpec((heads, total, hd), lambda i: (0, 0, 0)),
            pl.BlockSpec((kv_rows, 2 * hd), lambda i: (0, 0)),
        ),
        compiler_params=pltpu.CompilerParams(
            dimension_semantics=("arbitrary",), vmem_limit_bytes=60 * 1024 * 1024
        ),
    )(rows, *rest)


def attend_kernel(
    lift,
    q_in,
    kv_in,
    w_in,
    lat,
    gate,
    out,
    qbuf,
    kvbuf,
    acc,
    top,
    tot,
    osend,
    lsend,
    orecv,
    lrecv,
    orelay,
    lrelay,
    wfull,
    att,
    exch,
    ks,
    kr,
    qs,
    qr,
    ws,
    wr,
    os_,
    or_,
    ls_,
    lr_,
    ts,
    tr,
):
    z, x, y, c = (lax.axis_index(a) for a in ("z", "x", "y", "c"))
    me = y * NC + c
    zp, zm = lax.rem(z + 1, NZ), lax.rem(z + NZ - 1, NZ)
    xp, xm = lax.rem(x + 1, NX), lax.rem(x + NX - 1, NX)
    yp, ym = lax.rem(y + 1, NY), lax.rem(y + NY - 1, NY)
    heads, n, hd = q_in.shape
    n_ctx = kv_in.shape[0] - n
    scale = hd ** (-0.5) * math.log2(math.e)
    raw_lift = lift / hd ** (-0.5)
    t_to = tp_peers(y, c)
    greet([{"z": zp}, {"z": zm}, {"x": xp}, {"x": xm}] + t_to)

    started = []

    def go(*args, **to):
        cp = remote(*args, **to)
        cp.start()
        started.append(cp)
        return cp

    q1 = go(q_in, qbuf.at[1], qs.at[0], qr.at[0], x=xp)
    q2 = go(q_in, qbuf.at[2], qs.at[1], qr.at[1], x=xm)
    k1 = go(kv_in, kvbuf.at[1], ks.at[0], kr.at[0], z=zp)
    k2 = go(kv_in, kvbuf.at[2], ks.at[1], kr.at[1], z=zm)
    w1 = go(w_in, wfull.at[me], ws.at[0], wr.at[0], y=yp)
    w2 = go(w_in, wfull.at[me], ws.at[1], wr.at[1], y=ym)
    w0 = go(w_in, wfull.at[me], ws.at[2], wr.at[2], c=1 - c)

    qbuf[0] = q_in[...]
    kvbuf[0] = kv_in[...]
    wfull[me] = w_in[...]
    acc[...] = jnp.zeros_like(acc)
    tot[...] = jnp.zeros_like(tot)
    top[...] = jnp.full_like(top, -1e30)

    def update(a, h, k, v, add):
        s = lax.dot_general(qbuf[a, h], k, (((1,), (1,)), ((), ())), preferred_element_type=F32)
        if add:
            s = s + add
        wide = s.shape[1] // hd
        old = top[a, h]
        new = jnp.maximum(old, jnp.max(s, axis=1, keepdims=True))
        factor = jnp.exp2((old - new) * scale)
        p = jnp.exp2((s - jnp.concatenate([new] * wide, axis=1)) * scale)
        part = sum((p[:, i * hd : (i + 1) * hd] for i in range(1, wide)), p[:, 0:hd])
        top[a, h] = new
        tot[a, h] = tot[a, h] * factor + part
        acc[a, h] = acc[a, h] * factor + jnp.dot(p.astype(BF16), v, preferred_element_type=F32)

    def run(a0, na, b0, nb):
        def body(i, carry):
            b = b0 + lax.rem(i, nb)
            h = lax.rem(i // nb, heads)
            a = a0 + i // (nb * heads)
            update(a, h, kvbuf[b, 0:n, 0:hd], kvbuf[b, 0:n, hd : 2 * hd], 0.0)
            return carry

        lax.fori_loop(0, na * heads * nb, body, 0)

    def run_ctx(a0, na):
        def body(i, carry):
            kv = jnp.concatenate([kvbuf[b, n : n + n_ctx, :] for b in range(NZ)], axis=0)
            update(a0 + i // heads, lax.rem(i, heads), kv[:, 0:hd], kv[:, hd : 2 * hd], raw_lift)
            return carry

        lax.fori_loop(0, na * heads, body, 0)

    eye = diagonal(hd)
    blocks = n // hd

    def finish(a):
        def body(h, carry):
            total = jnp.sum(tot[a, h], axis=1, keepdims=True)
            osend[a - 1, h] = (acc[a, h] / total).astype(BF16)
            lse = top[a, h] * scale + jnp.log2(total)
            for b in range(blocks):
                row = jnp.sum(jnp.where(eye, lse[b * hd : (b + 1) * hd], 0.0), axis=0, keepdims=True)
                lsend[a - 1, h, b : b + 1, :] = row
            return carry

        lax.fori_loop(0, heads, body, 0)

    run(0, 1, 0, 1)
    q1.wait_recv()
    q2.wait_recv()
    q3 = go(qbuf.at[1, 0], qbuf.at[3, 0], qs.at[2], qr.at[2], x=xp)
    q4 = go(qbuf.at[2, 1], qbuf.at[3, 1], qs.at[3], qr.at[3], x=xm)
    k1.wait_recv()
    k2.wait_recv()
    k3 = go(kvbuf.at[1], kvbuf.at[3], ks.at[2], kr.at[2], z=zp)
    k4 = go(kvbuf.at[2], kvbuf.at[4], ks.at[3], kr.at[3], z=zm)
    run(1, 2, 0, 3)
    q3.wait_recv()
    q4.wait_recv()
    k3.wait_recv()
    k4.wait_recv()
    k5 = go(kvbuf.at[3], kvbuf.at[5], ks.at[4], kr.at[4], z=zp)
    k6 = go(kvbuf.at[4], kvbuf.at[6], ks.at[5], kr.at[5], z=zm)
    run(3, 1, 0, 3)
    run(1, 3, 3, 2)
    k5.wait_recv()
    k6.wait_recv()
    cut = n // 2
    k7 = go(kvbuf.at[5, 0:cut], kvbuf.at[7, 0:cut], ks.at[6], kr.at[6], z=zp)
    k8 = go(kvbuf.at[6, cut : n + n_ctx], kvbuf.at[7, cut : n + n_ctx], ks.at[7], kr.at[7], z=zm)
    run(0, 1, 1, 4)
    w1.wait_recv()
    w2.wait_recv()
    low, high, far = ym * NC + c, yp * NC + c, lax.rem(y + 2, NY) * NC + c
    wh = w_in.shape[0] // 2
    w3 = go(wfull.at[low, 0:wh], wfull.at[low, 0:wh], ws.at[3], wr.at[3], y=yp)
    w4 = go(wfull.at[high, wh : 2 * wh], wfull.at[high, wh : 2 * wh], ws.at[4], wr.at[4], y=ym)
    w5 = go(wfull.at[low], wfull.at[low], ws.at[5], wr.at[5], c=1 - c)
    w6 = go(wfull.at[high], wfull.at[high], ws.at[6], wr.at[6], c=1 - c)
    run(1, 3, 5, 2)
    k7.wait_recv()
    k8.wait_recv()
    run(3, 1, 7, 1)
    run_ctx(3, 1)
    finish(3)
    run(1, 1, 7, 1)
    o3 = go(osend.at[2, 0], orelay.at[0], os_.at[0], or_.at[0], x=xp)
    o4 = go(osend.at[2, 1], orelay.at[1], os_.at[1], or_.at[1], x=xm)
    l3 = go(lsend.at[2, 0], lrelay.at[0], ls_.at[0], lr_.at[0], x=xp)
    l4 = go(lsend.at[2, 1], lrelay.at[1], ls_.at[1], lr_.at[1], x=xm)
    run_ctx(1, 1)
    finish(1)
    run(2, 1, 7, 1)
    o1 = go(osend.at[0], orecv.at[0], os_.at[2], or_.at[2], x=xm)
    l1 = go(lsend.at[0], lrecv.at[0], ls_.at[2], lr_.at[2], x=xm)
    run_ctx(2, 1)
    finish(2)
    run(0, 1, 5, 1)
    o2 = go(osend.at[1], orecv.at[1], os_.at[3], or_.at[3], x=xp)
    l2 = go(lsend.at[1], lrecv.at[1], ls_.at[3], lr_.at[3], x=xp)
    for cp in (o3, o4, l3, l4):
        cp.wait_recv()
    o5 = go(orelay.at[0], orecv.at[2, 0], os_.at[4], or_.at[4], x=xp)
    o6 = go(orelay.at[1], orecv.at[2, 1], os_.at[5], or_.at[5], x=xm)
    l5 = go(lrelay.at[0], lrecv.at[2, 0], ls_.at[4], lr_.at[4], x=xp)
    l6 = go(lrelay.at[1], lrecv.at[2, 1], ls_.at[5], lr_.at[5], x=xm)
    run(0, 1, 6, 2)
    run_ctx(0, 1)
    w3.wait_recv()
    w4.wait_recv()
    w7 = go(wfull.at[far], wfull.at[far], ws.at[7], wr.at[7], c=1 - c)
    for cp in (o1, o2, o5, o6, l1, l2, l5, l6):
        cp.wait_recv()

    for h in range(heads):
        for b in range(blocks):
            at = slice(b * hd, (b + 1) * hd)
            total = jnp.sum(tot[0, h, at, :], axis=1, keepdims=True)
            lse = [top[0, h, at, :] + jnp.log2(total) * (1.0 / scale)]
            for i in range(NX - 1):
                row = jnp.broadcast_to(lrecv[i, h, b : b + 1, :], (hd, hd))
                col = jnp.sum(jnp.where(eye, row, 0.0), axis=1, keepdims=True)
                lse.append(jnp.broadcast_to(col * (1.0 / scale), (hd, hd)))
            best = functools.reduce(jnp.maximum, lse)
            weights = [jnp.exp2((v - best) * scale) for v in lse]
            summed = (acc[0, h, at, :] / total) * weights[0]
            for i in range(NX - 1):
                summed = summed + orecv[i, h, at, :].astype(F32) * weights[i + 1]
            att[at, h * hd : (h + 1) * hd] = (summed / sum(weights[1:], weights[0])).astype(BF16)

    mine = lat.shape[0]
    t_out = []
    for i, to in enumerate(t_to):
        at = pl.multiple_of(tp_index(to, y, c) * mine, mine)
        t_out.append(go(att.at[pl.ds(at, mine), :], exch.at[me], ts.at[i], tr.at[i], **to))
    exch[me] = att[pl.ds(pl.multiple_of(me * mine, mine), mine), :]
    for cp in (w0, w5, w6, w7):
        cp.wait_recv()
    for cp in t_out:
        cp.wait_recv()
    cols = 512
    d = lat.shape[1]
    rows_in = jnp.concatenate([exch[i] for i in range(NTP)], axis=1)
    for j in range(d // cols):
        sl = slice(j * cols, (j + 1) * cols)
        weight = wfull[:, :, sl].reshape(NTP * w_in.shape[0], cols)
        out[:, sl] = jnp.dot(rows_in, weight, preferred_element_type=F32)
    mixed = out[...]
    out[...] = lat[...].astype(F32) + gate[...] * rms(mixed)
    for cp in started:
        cp.wait_send()


def attend_stage(q, kv, w, lat, gate, lift):
    heads, n, hd = q.shape
    kv_rows = kv.shape[0]
    dma = pltpu.SemaphoreType.DMA
    mine, d = lat.shape
    return pl.pallas_call(
        functools.partial(attend_kernel, lift),
        name="attend_stage",
        out_shape=jax.ShapeDtypeStruct((mine, d), F32),
        in_specs=[VMEM_SPEC] * 5,
        out_specs=VMEM_SPEC,
        scratch_shapes=[
            pltpu.VMEM((NX, heads, n, hd), BF16),
            pltpu.VMEM((NZ, kv_rows, 2 * hd), BF16),
            pltpu.VMEM((NX, heads, n, hd), F32),
            pltpu.VMEM((NX, heads, n, hd), F32),
            pltpu.VMEM((NX, heads, n, hd), F32),
            pltpu.VMEM((NX - 1, heads, n, hd), BF16),
            pltpu.VMEM((NX - 1, heads, n // hd, hd), F32),
            pltpu.VMEM((NX - 1, heads, n, hd), BF16),
            pltpu.VMEM((NX - 1, heads, n // hd, hd), F32),
            pltpu.VMEM((heads, n, hd), BF16),
            pltpu.VMEM((heads, n // hd, hd), F32),
            pltpu.VMEM((NTP,) + w.shape, BF16),
            pltpu.VMEM((n, heads * hd), BF16),
            pltpu.VMEM((NTP, mine, heads * hd), BF16),
            dma((8,)),
            dma((8,)),
            dma((4,)),
            dma((4,)),
            dma((8,)),
            dma((8,)),
            dma((6,)),
            dma((6,)),
            dma((6,)),
            dma((6,)),
            dma((NTP - 1,)),
            dma((NTP - 1,)),
        ],
        compiler_params=pltpu.CompilerParams(
            collective_id=1, has_side_effects=True, vmem_limit_bytes=60 * 1024 * 1024
        ),
    )(q, kv, w, lat, gate)


def body(
    latents,
    context,
    cond,
    ctx_cond,
    mod_weight,
    query_weight,
    key_matrix,
    value_matrix,
    out_weight,
    query_gain,
    key_gain,
):
    d = latents.shape[1]
    rows, mod = gather_stage(latents, cond, ctx_cond, mod_weight)
    q, kv = project_stage(
        rows, context, mod, query_weight, key_matrix, value_matrix, query_gain, key_gain
    )
    tokens = latents.shape[0] * NTP * NZ * NX
    lift = math.log(tokens / (2.0 * context.shape[0] * NZ * NX))
    result = attend_stage(q, kv, out_weight, latents, mod[0:1, 2 * d :], lift)
    return result.astype(BF16)


def solution(mesh):
    torus = Mesh(mesh.devices.reshape(NZ, NX, NY, NC), ("z", "x", "y", "c"))
    sp, tp = ("z", "x"), ("y", "c")
    placed = (
        P(sp + tp, None),
        P(sp, None),
        P(sp),
        P(sp),
        P(sp, tp),
        P(None, tp),
        P(None, tp),
        P(None, tp),
        P(tp, None),
        P(),
        P(),
    )
    return jax.shard_map(body, mesh=torus, in_specs=placed, out_specs=P(sp + tp, None), check_vma=False)
```

time: 286 us -> 105 us (0.37)
  Pallas kernels: 0 us -> 102 us
  blocking collectives: 100 us -> 0 us
  waiting for transfers between devices: 70.3 us -> 0 us
  matrix products: 57.2 us -> 0 us
  other arithmetic: 22.9 us -> 1.77 us
  local copies, waits for them, and re-layouts: 20.4 us -> 1.32 us
  between operations: 13.4 us -> 0.02 us
    pallas_call x0 -> x3, Pallas kernels: none -> 102 us  [the longest x1 70.4 us: attend_stage(): pl.pallas_call(functools.partial(attend_kernel, lift), name='attend_stage...]
    all_gather x3 -> x0, waiting for transfers between devices: 69.5 us -> none  [the longest x1 46.4 us: side_by_side(): filled, at, done = (lax.all_gather(both, axis, axis=dim, tiled=True), 0, [])]
    all_gather x2 -> x0, blocking collectives: 59.9 us -> none  [the longest x1 40.4 us: side_by_side(): filled, at, done = (lax.all_gather(both, axis, axis=dim, tiled=True), 0, [])]
    dot_general x25 -> x0, matrix products: 57.2 us -> none  [the longest x8 22.2 us: update(): jnp.einsum('hqk,khd->hqd', weights_now.astype(jnp.bfloat16), value_block,...]
    psum x2 -> x0, blocking collectives: 26.1 us -> none  [over_axes(): value = lax.psum(value, axis)]
    all_to_all x1 -> x0, blocking collectives: 14.5 us -> none  [body(): lax.all_to_all(attended, 'tp', split_axis=0, concat_axis=1, tiled=True)]
    reduce_sum x11 -> x0, other arithmetic: 13.1 us -> none  [the longest x8 11.5 us: update(): jnp.sum(weights_now, axis=-1)]
    while x10 -> x0, local copies, waits for them, and re-layouts: 12.8 us -> none  [the longest x2 12.8 us: body(): state_out, _ = lax.scan(one_step, initial, (key_blocks, value_blocks))]
  transfers between devices with their start and end apart: 3 -> 0, of which waited for: 2 -> 0; matrix products, arithmetic and copies ran while one was open for 29% -> 0% of each run, Pallas kernels for 0% -> 0%
where the time goes in v1:
time: 105 us
  Pallas kernels  102 us (97%)
  other arithmetic  1.77 us (2%)
  local copies, waits for them, and re-layouts  1.32 us (1%)
    pallas_call x1, Pallas kernels, attend_stage(): pl.pallas_call(functools.partial(attend_kernel, lift), name='attend_stage...  70.4 us
    pallas_call x1, Pallas kernels, gather_stage(): pl.pallas_call(gather_kernel, name='gather_stage', out_shape=(jax.ShapeDt...  25.4 us
    pallas_call x1, Pallas kernels, project_stage(): pl.pallas_call(project_kernel, name='project_stage', grid=(steps,), out_s...  5.75 us

profile of v1, /device:TPU:1, one launch (start us, length us, event | category | flops | bytes accessed | tf_op | source)
XLA Modules:
  0.0 104.7 jit_solution(8672796168825753)
XLA Ops:
  0.0 25.4 %gather_stage.1 = (bf16[8,64,2048]{2,1,0:T(8,128)(2,1)}, f32[2,6144]{1,0:T(2,128)}) custom-call(bf16[64,2048]{1,0:T(8,128)(2,1)} %lat.3, f32[1,64]{1,0:T(1,128)} %bitcast.4, f32[1,64]{1,0:T(1,128)} %bitcast.5, f32[64,768]{1,0:T(8,128)} %mod_weight.1), custom_call_target="tpu_custom_call" | custom-call | tf_op jit(solution)/shard_map/gather_stage/pallas_call | solution.py:136
  25.4 5.8 %project_stage.1 = (bf16[2,512,128]{2,1,0:T(8,128)(2,1)}, bf16[528,256]{1,0:T(8,128)(2,1)}) custom-call(bf16[8,64,2048]{2,1,0:T(8,128)(2,1)} %get-tuple-element.9.rows, bf16[16,2048]{1,0:T(8,128)(2,1)} %ctx.1, f32[2,6144]{1,0:T(2,128)} %get-tuple-element.10.mod, bf16[2048,256]{1,0:T(8,128)(2,1)} %wq.1, bf16[2048,128]{1,0:T(8,128)(2,1)} %wk.1, ...), custom_call_target="tpu_custom_call" | custom-call | tf_op jit(solution)/shard_map/project_stage/pallas_call | solution.py:239
  31.2 1.3 %slice.3.gate = f32[1,2048]{1,0:T(1,128)} slice(f32[2,6144]{1,0:T(2,128)} %get-tuple-element.10.mod), slice={[0:1], [4096:6144]} | slice | bytes 16384 | tf_op jit(solution)/shard_map/slice | solution.py:546
  32.5 70.4 %attend_stage.1 = f32[64,2048]{1,0:T(8,128)} custom-call(bf16[2,512,128]{2,1,0:T(8,128)(2,1)} %get-tuple-element.11.q_in, bf16[528,256]{1,0:T(8,128)(2,1)} %get-tuple-element.12.kv_in, bf16[256,2048]{1,0:T(8,128)(2,1)} %w_in.1, bf16[64,2048]{1,0:T(8,128)(2,1)} %lat.3, f32[1,2048]{1,0:T(1,128)} %slice.3.gate), custom_call_target="tpu_custom_call" | custom-call | tf_op jit(solution)/shard_map/attend_stage/pallas_call | solution.py:486
  102.9 1.8 %convert_element_type.3 = bf16[64,2048]{1,0:T(8,128)(2,1)} convert(f32[64,2048]{1,0:T(8,128)} %attend_stage.1) | non-fusion elementwise | flops 131072 | bytes 786432 | tf_op jit(solution)/shard_map/convert_element_type | solution.py:547

commit v2 on v0

v2 whole, which is shorter than its diff:
```python
import functools
import math

import jax
import jax.numpy as jnp
import numpy as np
from jax import lax
from jax.experimental import pallas as pl
from jax.experimental.pallas import tpu as pltpu
from jax.sharding import Mesh
from jax.sharding import PartitionSpec as P

MESH_ID = pl.DeviceIdType.MESH
GRID_W = 64
NORM_EPS = 1e-06
ROPE_BASE = 10000.0
NZ, NX, NY, NC = 8, 4, 4, 2
NTP = NY * NC
BF16, F32 = jnp.bfloat16, jnp.float32
VMEM_SPEC = pl.BlockSpec(memory_space=pltpu.VMEM)


def remote(src, dst, send_sem, recv_sem, **to):
    return pltpu.make_async_remote_copy(
        src_ref=src,
        dst_ref=dst,
        send_sem=send_sem,
        recv_sem=recv_sem,
        device_id=to,
        device_id_type=MESH_ID,
    )


class View:
    def __init__(self, ref, index=None):
        self.ref, self.index = ref, index

    def __getitem__(self, index):
        return View(self.ref, index)


def make(*args, **to):
    return remote(*(a.ref.at[a.index] if isinstance(a, View) else a for a in args), **to)


def greet(peers):
    barrier = pltpu.get_barrier_semaphore()
    for peer in peers:
        pl.semaphore_signal(barrier, inc=1, device_id=peer, device_id_type=MESH_ID)
    pl.semaphore_wait(barrier, len(peers))


def tp_peers(y, c):
    peers = [{"c": 1 - c}]
    for dy in range(1, NY):
        for dc in range(NC):
            peers.append({"y": lax.rem(y + dy, NY), "c": lax.rem(c + dc, NC)})
    return peers


def tp_index(peer, y, c):
    return peer.get("y", y) * NC + peer["c"]


def diagonal(n):
    return lax.broadcasted_iota(jnp.int32, (n, n), 0) == lax.broadcasted_iota(jnp.int32, (n, n), 1)


def rope_tables(row_tokens, freqs):
    c = freqs // 4
    inv = (ROPE_BASE ** (-np.arange(c, dtype=np.float32) / np.float32(c))).astype(np.float32)

    def table(count, lanes_from):
        angles = np.arange(count, dtype=np.float32)[:, None] * inv[None, :]
        cos, sin = np.cos(angles), np.sin(angles)
        out_c = np.zeros((count, freqs), np.float32)
        out_s = np.zeros((count, freqs), np.float32)
        out_c[:, lanes_from : lanes_from + 2 * c] = np.concatenate([cos, cos], 1)
        out_s[:, lanes_from : lanes_from + 2 * c] = np.concatenate([-sin, sin], 1)
        return out_c, out_s

    return table(row_tokens, 0) + table(GRID_W, freqs // 2)


def rms(v):
    return v * lax.rsqrt(jnp.mean(v * v, axis=-1, keepdims=True) + NORM_EPS)


def block_kernel(
    lift,
    lat,
    ctx,
    cond,
    ctx_cond,
    mod_weight,
    qg,
    kg,
    row_c,
    row_s,
    col_c,
    col_s,
    wq_hbm,
    wk_hbm,
    wv_hbm,
    w_hbm,
    out,
    rows,
    normed,
    mod,
    part,
    px,
    pt,
    zbuf,
    xbuf,
    tbuf,
    wq,
    wkv,
    qbuf,
    kvbuf,
    cbuf,
    acc,
    top,
    tot,
    osend,
    lsend,
    orecv,
    lrecv,
    orelay,
    lrelay,
    wfull,
    att,
    exch,
    mixed,
    loc,
    rs,
    rr,
    zs,
    zr,
    xs,
    xr,
    ms,
    mr,
    ks,
    kr,
    qs,
    qr,
    ws,
    wr,
    os_,
    or_,
    ls_,
    lr_,
    ts,
    tr,
):
    z, x, y, c = (lax.axis_index(a) for a in ("z", "x", "y", "c"))
    me = y * NC + c
    zp, zm = lax.rem(z + 1, NZ), lax.rem(z + NZ - 1, NZ)
    xp, xm = lax.rem(x + 1, NX), lax.rem(x + NX - 1, NX)
    yp, ym = lax.rem(y + 1, NY), lax.rem(y + NY - 1, NY)
    low, high, far = ym * NC + c, yp * NC + c, lax.rem(y + 2, NY) * NC + c
    mine, d = lat.shape
    heads, n, hd = qbuf.shape[1:]
    n_ctx = ctx.shape[0]
    scale = hd ** (-0.5) * math.log2(math.e)
    raw_lift = lift / hd ** (-0.5)

    fetch = [
        pltpu.make_async_copy(wk_hbm, wkv.at[:, 0:hd], loc.at[0]),
        pltpu.make_async_copy(wv_hbm, wkv.at[:, hd : 2 * hd], loc.at[1]),
        pltpu.make_async_copy(wq_hbm, wq, loc.at[2]),
        pltpu.make_async_copy(w_hbm, wfull.at[me], loc.at[3]),
    ]
    for cp in fetch:
        cp.start()

    z_to = [{"z": lax.rem(z + i, NZ)} for i in range(1, NZ)]
    x_to = [{"x": lax.rem(x + i, NX)} for i in range(1, NX)]
    t_to = tp_peers(y, c)
    greet(z_to + x_to + t_to)

    started = []

    def go(*args, **to):
        cp = functools.partial(make, *args, **to)
        cp().start()
        started.append(cp)
        return cp

    def got(copies):
        for cp in copies:
            cp().wait_recv()

    rh = mine // 2
    rpiece = (pl.ds(0, rh), pl.ds(rh, rh))

    def r_to(src, row, p, i, **to):
        return go(src, View(rows)[row, rpiece[p]], View(rs)[i], View(rr)[i], **to)

    up = [r_to(View(lat)[rpiece[p]], me, p, p, y=yp) for p in (0, 1)]
    down = [r_to(View(lat)[rpiece[p]], me, p, 2 + p, y=ym) for p in (1, 0)]
    across = [go(lat, View(rows)[me], View(rs)[6], View(rr)[6], c=1 - c)]

    eye_in = diagonal(cond.shape[1])
    for r, ref in enumerate((cond, ctx_cond)):
        v = ref[...]
        v = v * jax.nn.sigmoid(v)
        column = jnp.sum(jnp.where(eye_in, jnp.broadcast_to(v, eye_in.shape), 0.0), axis=1, keepdims=True)
        part[r : r + 1, :] = jnp.sum(column * mod_weight[...], axis=0, keepdims=True)
    z_out = [go(part, View(zbuf)[z], View(zs)[i], View(zr)[i], **to) for i, to in enumerate(z_to)]
    zbuf[z] = part[...]
    rows[me] = lat[...]
    acc[...] = jnp.zeros_like(acc)
    tot[...] = jnp.zeros_like(tot)
    top[...] = jnp.full_like(top, -1e30)
    got(z_out)
    px[...] = sum((zbuf[i] for i in range(1, NZ)), zbuf[0])
    x_out = [go(px, View(xbuf)[x], View(xs)[i], View(xr)[i], **to) for i, to in enumerate(x_to)]
    xbuf[x] = px[...]
    got([up[0], down[0]])
    up2 = r_to(View(rows)[low, rpiece[0]], low, 0, 4, y=yp)
    down2 = r_to(View(rows)[high, rpiece[1]], high, 1, 5, y=ym)
    got(x_out)
    pt[...] = sum((xbuf[i] for i in range(1, NX)), xbuf[0])
    m_out = [go(pt, View(tbuf)[me], View(ms)[i], View(mr)[i], **to) for i, to in enumerate(t_to)]
    tbuf[me] = pt[...]
    got([up[1], down[1]])
    across.append(go(View(rows)[low], View(rows)[low], View(rs)[7], View(rr)[7], c=1 - c))
    across.append(go(View(rows)[high], View(rows)[high], View(rs)[8], View(rr)[8], c=1 - c))
    got([up2, down2])
    across.append(go(View(rows)[far], View(rows)[far], View(rs)[9], View(rr)[9], c=1 - c))
    for cp in fetch:
        cp.wait()

    wh = w_hbm.shape[0] // 2
    wpiece = (pl.ds(0, wh), pl.ds(wh, wh))

    def w_to(row, p, i, **to):
        piece = View(wfull)[row, wpiece[p]]
        return go(piece, piece, View(ws)[i], View(wr)[i], **to)

    w1 = [w_to(me, p, p, y=yp) for p in (0, 1)]
    w2 = [w_to(me, p, 2 + p, y=ym) for p in (1, 0)]
    w0 = go(View(wfull)[me], View(wfull)[me], View(ws)[8], View(wr)[8], c=1 - c)
    got(m_out)
    w = part.shape[1]
    for i in range(NTP):
        mod[:, i * w : (i + 1) * w] = tbuf[i]
    got(across)

    cut = n // 2
    kpiece = (pl.ds(0, cut), pl.ds(cut, cut + n_ctx))

    def k_to(src, slot, p, **to):
        i = 2 * (slot - 1) + p
        return go(View(kvbuf)[src, kpiece[p]], View(kvbuf)[slot, kpiece[p]], View(ks)[i], View(kr)[i], **to)

    def q_to(src, slot, h, **to):
        i = 2 * (slot - 1) + h
        return go(View(qbuf)[src, h], View(qbuf)[slot, h], View(qs)[i], View(qr)[i], **to)

    def modulated(v, r):
        v = rms(v.astype(F32))
        return (v * (1.0 + mod[r : r + 1, d : 2 * d]) + mod[r : r + 1, 0:d]).astype(BF16)

    groups = cut // GRID_W
    first = (z * NX + x) * (n // GRID_W)
    lane = lax.broadcasted_iota(jnp.int32, (cut, hd), 1)
    early = lax.rem(lane, hd // 2) < hd // 4

    def table(row_table, col_table, i):
        at = [first + i * groups + g for g in range(groups)]
        return jnp.concatenate([row_table[pl.ds(t, 1), :] + col_table[...] for t in at], axis=0)

    def turned(v, i):
        other = jnp.where(early, pltpu.roll(v, hd - hd // 4, 1), pltpu.roll(v, hd // 4, 1))
        return (v * table(row_c, col_c, i) + other * table(row_s, col_s, i)).astype(BF16)

    k1, k2 = [], []
    per = NTP // 2
    for i in range(2):
        for g in range(per):
            normed[i * per + g] = modulated(rows[i * per + g], 0)
        a = normed[i * per : (i + 1) * per].reshape(cut, d)
        kv = jnp.dot(a, wkv[...], preferred_element_type=F32)
        at = slice(i * cut, (i + 1) * cut)
        kvbuf[0, at, 0:hd] = turned(rms(kv[:, 0:hd]) * kg[...], i)
        kvbuf[0, at, hd : 2 * hd] = kv[:, hd : 2 * hd].astype(BF16)
        if i == 1:
            kv = jnp.dot(modulated(ctx[...], 1), wkv[...], preferred_element_type=F32)
            kvbuf[0, n : n + n_ctx, 0:hd] = (rms(kv[:, 0:hd]) * kg[...]).astype(BF16)
            kvbuf[0, n : n + n_ctx, hd : 2 * hd] = kv[:, hd : 2 * hd].astype(BF16)
        k1.append(k_to(0, 1, i, z=zp))
        k2.append(k_to(0, 2, i, z=zm))
    for i in range(2):
        a = normed[i * per : (i + 1) * per].reshape(cut, d)
        q = jnp.dot(a, wq[...], preferred_element_type=F32)
        for h in range(heads):
            at = slice(i * cut, (i + 1) * cut)
            qbuf[0, h, at, :] = turned(rms(q[:, h * hd : (h + 1) * hd]) * qg[...], i)
    q1 = [q_to(0, 1, h, x=xp) for h in (0, 1)]
    q2 = [q_to(0, 2, h, x=xm) for h in (1, 0)]

    def scores(a, h, k):
        return lax.dot_general(qbuf[a, h], k, (((1,), (1,)), ((), ())), preferred_element_type=F32)

    def update(a, h, s, v):
        wide = s.shape[1] // hd
        old = top[a, h]
        new = jnp.maximum(old, jnp.max(s, axis=1, keepdims=True))
        factor = jnp.exp2((old - new) * scale)
        p = jnp.exp2((s - jnp.concatenate([new] * wide, axis=1)) * scale)
        some = sum((p[:, i * hd : (i + 1) * hd] for i in range(1, wide)), p[:, 0:hd])
        top[a, h] = new
        tot[a, h] = tot[a, h] * factor + some
        acc[a, h] = acc[a, h] * factor + jnp.dot(p.astype(BF16), v, preferred_element_type=F32)

    def tile(a, slots, tail=False):
        more = [cbuf[...]] if tail else []
        m = n * len(slots)
        k = jnp.concatenate([kvbuf[b, 0:n, 0:hd] for b in slots] + [e[:, 0:hd] for e in more], axis=0)
        v = jnp.concatenate([kvbuf[b, 0:n, hd : 2 * hd] for b in slots] + [e[:, hd : 2 * hd] for e in more], axis=0)
        found = [scores(a, h, k) for h in range(heads)]
        for h in range(heads):
            s = found[h]
            if tail:
                s = jnp.concatenate([s[:, 0:m], s[:, m:] + raw_lift], axis=1)
            update(a, h, s, v)

    eye = diagonal(hd)
    blocks = n // hd

    def join(a, h, others, o_to, l_to):
        for b in range(blocks):
            at = pl.ds(b * hd, hd)
            total = jnp.sum(tot[a, h, at, :], axis=1, keepdims=True)
            value = acc[a, h, at, :] / total
            lse = top[a, h, at, :] * scale + jnp.log2(total)
            if others:
                lses, values = [lse], [value]
                for o_ref, l_ref in others:
                    row = jnp.broadcast_to(l_ref[b : b + 1, :], (hd, hd))
                    col = jnp.sum(jnp.where(eye, row, 0.0), axis=1, keepdims=True)
                    lses.append(jnp.broadcast_to(col, (hd, hd)))
                    values.append(o_ref[at, :].astype(F32))
                best = functools.reduce(jnp.maximum, lses)
                weights = [jnp.exp2(v - best) for v in lses]
                total = sum(weights[1:], weights[0])
                value = sum((w * v for w, v in zip(weights[1:], values[1:])), weights[0] * values[0]) / total
                lse = best + jnp.log2(total)
            o_to(b, value.astype(BF16))
            if l_to is not None:
                l_to[b : b + 1, :] = jnp.sum(jnp.where(eye, lse, 0.0), axis=0, keepdims=True)

    def finish(a, h, others=()):
        def put(b, value):
            osend[a - 1, h, b * hd : (b + 1) * hd, :] = value

        join(a, h, others, put, lsend.at[a - 1, h])

    def o_go(a, h, to_o, to_l, i, **to):
        ls = go(View(lsend)[a - 1, h], to_l, View(ls_)[i], View(lr_)[i], **to)
        return [ls, go(View(osend)[a - 1, h], to_o, View(os_)[i], View(or_)[i], **to)]

    k3, k4, k5, k6, k7, q34, w34 = [], [], [], [], [], [], []
    got([k1[0], k2[0]])
    k3.append(k_to(1, 3, 0, z=zp))
    k4.append(k_to(2, 4, 0, z=zm))
    got([k1[1], k2[1]])
    k3.append(k_to(1, 3, 1, z=zp))
    k4.append(k_to(2, 4, 1, z=zm))
    got([q1[0], q2[0]])
    q34.append(q_to(1, 3, 0, x=xp))
    q34.append(q_to(2, 3, 1, x=xm))
    got([q1[1], q2[1]])

    def one(j, carry):
        @pl.when(j == 1)
        def _():
            got([k3[0], k4[0]])
            k5.append(k_to(3, 5, 0, z=zp))
            k6.append(k_to(4, 6, 0, z=zm))

        @pl.when(j == 3)
        def _():
            got([k3[1], k4[1]])
            k5.append(k_to(3, 5, 1, z=zp))
            k6.append(k_to(4, 6, 1, z=zm))
            got(q34)

        tile(jnp.where(j == 2, 0, jnp.where(j == 3, 3, j + 1)), (0, 1, 2))
        return carry

    lax.fori_loop(0, 4, one, 0)

    def two(j, carry):
        @pl.when(j == 0)
        def _():
            got([k5[0], k6[0]])
            k7.append(k_to(5, 7, 0, z=zp))
            got([w1[0], w2[0]])
            w34.append(w_to(low, 0, 4, y=yp))
            w34.append(w_to(high, 1, 5, y=ym))

        @pl.when(j == 2)
        def _():
            got([k5[1], k6[1]])
            k7.append(k_to(6, 7, 1, z=zm))

        tile(jnp.where(j == 3, 0, j + 1), (3, 4))
        return carry

    lax.fori_loop(0, 4, two, 0)
    got(k7)
    for b in range(NZ):
        cbuf[b * n_ctx : (b + 1) * n_ctx, :] = kvbuf[b, n : n + n_ctx, :]

    late = (5, 6, 7)
    tile(3, late, True)
    finish(3, 0)
    finish(3, 1)
    far0 = o_go(3, 0, View(orelay)[0], View(lrelay)[0], 0, x=xp)
    far1 = o_go(3, 1, View(orelay)[1], View(lrelay)[1], 1, x=xm)

    def near(a, carry):
        tile(a, late, True)
        return carry

    lax.fori_loop(1, 3, near, 0)
    finish(1, 0)
    finish(2, 1)
    pure0 = o_go(1, 0, View(orecv)[1, 0], View(lrecv)[1, 0], 2, x=xm)
    pure1 = o_go(2, 1, View(orecv)[0, 1], View(lrecv)[0, 1], 3, x=xp)
    got([w1[1], w2[1]])
    w5 = go(View(wfull)[low], View(wfull)[low], View(ws)[6], View(wr)[6], c=1 - c)
    w6 = go(View(wfull)[high], View(wfull)[high], View(ws)[7], View(wr)[7], c=1 - c)
    got(far0 + far1)
    finish(2, 0, [(orelay.at[0], lrelay.at[0])])
    finish(1, 1, [(orelay.at[1], lrelay.at[1])])
    both0 = o_go(2, 0, View(orecv)[0, 0], View(lrecv)[0, 0], 4, x=xp)
    both1 = o_go(1, 1, View(orecv)[1, 1], View(lrecv)[1, 1], 5, x=xm)
    tile(0, late, True)
    got(w34)
    w7 = go(View(wfull)[far], View(wfull)[far], View(ws)[9], View(wr)[9], c=1 - c)
    got(pure0 + pure1 + both0 + both1)

    for h in range(heads):

        def put(b, value, h=h):
            att[b * hd : (b + 1) * hd, h * hd : (h + 1) * hd] = value

        join(0, h, [(orecv.at[i, h], lrecv.at[i, h]) for i in range(2)], put, None)

    t_out = [None] * len(t_to)
    for i in (3, 4, 1, 2, 5, 6, 0):
        at = pl.multiple_of(tp_index(t_to[i], y, c) * mine, mine)
        t_out[i] = go(View(att)[pl.ds(at, mine), :], View(exch)[me], View(ts)[i], View(tr)[i], **t_to[i])
    exch[me] = att[pl.ds(pl.multiple_of(me * mine, mine), mine), :]

    def add(source, fresh=False):
        product = jnp.dot(exch[source], wfull[source], preferred_element_type=F32)
        mixed[...] = product if fresh else mixed[...] + product

    def came(i):
        got([t_out[i]])
        back = {1: 5, 2: 6, 5: 1, 6: 2}.get(i, i)
        add(tp_index(t_to[back], y, c))

    add(me, True)
    got([w0])
    came(0)
    got([w5, w6])
    for i in (1, 2, 5, 6):
        came(i)
    got([w7])
    for i in (3, 4):
        came(i)
    out[...] = (lat[...].astype(F32) + mod[0:1, 2 * d : 3 * d] * rms(mixed[...])).astype(BF16)
    for cp in started:
        cp().wait_send()


def body(
    latents,
    context,
    cond,
    ctx_cond,
    mod_weight,
    query_weight,
    key_matrix,
    value_matrix,
    out_weight,
    query_gain,
    key_gain,
):
    mine, d = latents.shape
    n_ctx = context.shape[0]
    hd = query_gain.shape[0]
    heads = query_weight.shape[1] // hd
    n = mine * NTP
    kv_rows = n + n_ctx
    cols = mod_weight.shape[1]
    tokens = n * NZ * NX
    lift = math.log(tokens / (2.0 * n_ctx * NZ * NX))
    tables = [jnp.asarray(t) for t in rope_tables(tokens // GRID_W, hd)]
    dma = pltpu.SemaphoreType.DMA
    pairs = [s for count in (10, NZ - 1, NX - 1, NTP - 1, 14, 6, 10, 6, 6, NTP - 1) for s in (dma((count,)),) * 2]
    return pl.pallas_call(
        functools.partial(block_kernel, lift),
        name="block_stage",
        out_shape=jax.ShapeDtypeStruct((mine, d), BF16),
        in_specs=[VMEM_SPEC] * 11 + [pl.BlockSpec(memory_space=pl.ANY)] * 4,
        out_specs=VMEM_SPEC,
        scratch_shapes=[
            pltpu.VMEM((NTP, mine, d), BF16),
            pltpu.VMEM((NTP, mine, d), BF16),
            pltpu.VMEM((2, NTP * cols), F32),
            pltpu.VMEM((2, cols), F32),
            pltpu.VMEM((2, cols), F32),
            pltpu.VMEM((2, cols), F32),
            pltpu.VMEM((NZ, 2, cols), F32),
            pltpu.VMEM((NX, 2, cols), F32),
            pltpu.VMEM((NTP, 2, cols), F32),
            pltpu.VMEM(query_weight.shape, BF16),
            pltpu.VMEM((d, 2 * hd), BF16),
            pltpu.VMEM((NX, heads, n, hd), BF16),
            pltpu.VMEM((NZ, kv_rows, 2 * hd), BF16),
            pltpu.VMEM((NZ * n_ctx, 2 * hd), BF16),
            pltpu.VMEM((NX, heads, n, hd), F32),
            pltpu.VMEM((NX, heads, n, hd), F32),
            pltpu.VMEM((NX, heads, n, hd), F32),
            pltpu.VMEM((NX - 1, heads, n, hd), BF16),
            pltpu.VMEM((NX - 1, heads, n // hd, hd), F32),
            pltpu.VMEM((2, heads, n, hd), BF16),
            pltpu.VMEM((2, heads, n // hd, hd), F32),
            pltpu.VMEM((2, n, hd), BF16),
            pltpu.VMEM((2, n // hd, hd), F32),
            pltpu.VMEM((NTP,) + out_weight.shape, BF16),
            pltpu.VMEM((n, heads * hd), BF16),
            pltpu.VMEM((NTP, mine, heads * hd), BF16),
            pltpu.VMEM((mine, d), F32),
            dma((4,)),
        ]
        + pairs,
        compiler_params=pltpu.CompilerParams(
            collective_id=0, has_side_effects=True, vmem_limit_bytes=62 * 1024 * 1024
        ),
    )(
        latents,
        context,
        cond[None, :],
        ctx_cond[None, :],
        mod_weight,
        query_gain[None, :],
        key_gain[None, :],
        *tables,
        query_weight,
        key_matrix,
        value_matrix,
        out_weight,
    )


def solution(mesh):
    torus = Mesh(mesh.devices.reshape(NZ, NX, NY, NC), ("z", "x", "y", "c"))
    sp, tp = ("z", "x"), ("y", "c")
    placed = (
        P(sp + tp, None),
        P(sp, None),
        P(sp),
        P(sp),
        P(sp, tp),
        P(None, tp),
        P(None, tp),
        P(None, tp),
        P(tp, None),
        P(),
        P(),
    )
    return jax.shard_map(body, mesh=torus, in_specs=placed, out_specs=P(sp + tp, None), check_vma=False)
```

time: 286 us -> 77.7 us (0.27)
  blocking collectives: 100 us -> 0 us
  Pallas kernels: 0 us -> 75.8 us
  waiting for transfers between devices: 70.3 us -> 0 us
  matrix products: 57.2 us -> 0 us
  other arithmetic: 22.9 us -> 0 us
  local copies, waits for them, and re-layouts: 20.4 us -> 1.67 us
  between operations: 13.4 us -> 0.01 us
    pallas_call x0 -> x1, Pallas kernels: none -> 75.8 us  [body(): pl.pallas_call(functools.partial(block_kernel, lift), name='block_stage',...]
    all_gather x3 -> x0, waiting for transfers between devices: 69.5 us -> none  [the longest x1 46.4 us: side_by_side(): filled, at, done = (lax.all_gather(both, axis, axis=dim, tiled=True), 0, [])]
    all_gather x2 -> x0, blocking collectives: 59.9 us -> none  [the longest x1 40.4 us: side_by_side(): filled, at, done = (lax.all_gather(both, axis, axis=dim, tiled=True), 0, [])]
    dot_general x25 -> x0, matrix products: 57.2 us -> none  [the longest x8 22.2 us: update(): jnp.einsum('hqk,khd->hqd', weights_now.astype(jnp.bfloat16), value_block,...]
    psum x2 -> x0, blocking collectives: 26.1 us -> none  [over_axes(): value = lax.psum(value, axis)]
    all_to_all x1 -> x0, blocking collectives: 14.5 us -> none  [body(): lax.all_to_all(attended, 'tp', split_axis=0, concat_axis=1, tiled=True)]
    reduce_sum x11 -> x0, other arithmetic: 13.1 us -> none  [the longest x8 11.5 us: update(): jnp.sum(weights_now, axis=-1)]
    while x10 -> x0, local copies, waits for them, and re-layouts: 12.8 us -> none  [the longest x2 12.8 us: body(): state_out, _ = lax.scan(one_step, initial, (key_blocks, value_blocks))]
  transfers between devices with their start and end apart: 3 -> 0, of which waited for: 2 -> 0; matrix products, arithmetic and copies ran while one was open for 29% -> 0% of each run, Pallas kernels for 0% -> 0%
where the time goes in v2:
time: 77.7 us; the launch traced here: 77.5 us
  Pallas kernels  75.8 us (98%)
  local copies, waits for them, and re-layouts  1.67 us (2%)
    pallas_call x1, Pallas kernels, body(): pl.pallas_call(functools.partial(block_kernel, lift), name='block_stage',...  75.8 us
    unnamed x1, local copies, waits for them, and re-layouts  1.67 us

profile of v2, /device:TPU:1, one launch (start us, length us, event | category | flops | bytes accessed | tf_op | source)
XLA Modules:
  0.0 77.5 jit_solution(6447669260091835806)
XLA Ops:
  0.0 75.8 %block_stage.1 = bf16[64,2048]{1,0:T(8,128)(2,1)} custom-call(bf16[64,2048]{1,0:T(8,128)(2,1)} %lat.1, bf16[16,2048]{1,0:T(8,128)(2,1)} %ctx.1, f32[1,64]{1,0:T(1,128)} %bitcast.4, f32[1,64]{1,0:T(1,128)} %bitcast.5, f32[64,768]{1,0:T(8,128)} %mod_weight.1, f32[1,128]{1,0:T(1,128)} %bitcast.6, f32[1,128]{1,0:T(1,128)} %bitcast.7, ...), custom_call_target="tpu_custom_call" | custom-call | tf_op jit(solution)/shard_map/block_stage/pallas_call | solution.py:508
  75.9 1.7 %copy.17 = bf16[64,2048]{1,0:T(8,128)(2,1)} copy(bf16[64,2048]{1,0:T(8,128)(2,1)} %block_stage.1) | data formatting | bytes 524288

commit v3 on v2

--- a/solution.py
+++ b/solution.py
@@ -47,7 +47,7 @@
     barrier = pltpu.get_barrier_semaphore()
     for peer in peers:
         pl.semaphore_signal(barrier, inc=1, device_id=peer, device_id_type=MESH_ID)
-    pl.semaphore_wait(barrier, len(peers))
+    return functools.partial(pl.semaphore_wait, barrier, len(peers))
 
 
 def tp_peers(y, c):
@@ -88,22 +88,29 @@
 
 def block_kernel(
     lift,
-    lat,
-    ctx,
-    cond,
-    ctx_cond,
-    mod_weight,
-    qg,
-    kg,
-    row_c,
-    row_s,
-    col_c,
-    col_s,
-    wq_hbm,
-    wk_hbm,
-    wv_hbm,
-    w_hbm,
-    out,
+    *refs,
+):
+    (
+        lat_hbm,
+        ctx_hbm,
+        cond_hbm,
+        ctx_cond_hbm,
+        mod_weight_hbm,
+        qg_hbm,
+        kg_hbm,
+        row_c_hbm,
+        row_s_hbm,
+        col_c_hbm,
+        col_s_hbm,
+        wq_hbm,
+        wk_hbm,
+        wv_hbm,
+        w_hbm,
+        out,
+        *refs,
+    ) = refs
+    (lat, ctx, cond, ctx_cond, mod_weight, qg, kg, row_c, row_s, col_c, col_s, *refs) = refs
+    (
     rows,
     normed,
     mod,
@@ -152,7 +159,7 @@
     lr_,
     ts,
     tr,
-):
+    ) = refs
     z, x, y, c = (lax.axis_index(a) for a in ("z", "x", "y", "c"))
     me = y * NC + c
     zp, zm = lax.rem(z + 1, NZ), lax.rem(z + NZ - 1, NZ)
@@ -165,19 +172,34 @@
     scale = hd ** (-0.5) * math.log2(math.e)
     raw_lift = lift / hd ** (-0.5)
 
-    fetch = [
-        pltpu.make_async_copy(wk_hbm, wkv.at[:, 0:hd], loc.at[0]),
-        pltpu.make_async_copy(wv_hbm, wkv.at[:, hd : 2 * hd], loc.at[1]),
-        pltpu.make_async_copy(wq_hbm, wq, loc.at[2]),
-        pltpu.make_async_copy(w_hbm, wfull.at[me], loc.at[3]),
-    ]
-    for cp in fetch:
-        cp.start()
 
     z_to = [{"z": lax.rem(z + i, NZ)} for i in range(1, NZ)]
     x_to = [{"x": lax.rem(x + i, NX)} for i in range(1, NX)]
     t_to = tp_peers(y, c)
-    greet(z_to + x_to + t_to)
+    greeted = greet(z_to + x_to + t_to)
+
+    fetches = (
+        (lat_hbm, lat),
+        (mod_weight_hbm, mod_weight),
+        (cond_hbm, cond),
+        (ctx_cond_hbm, ctx_cond),
+        (wk_hbm, wkv.at[:, 0:hd]),
+        (wv_hbm, wkv.at[:, hd : 2 * hd]),
+        (ctx_hbm, ctx),
+        (row_c_hbm, row_c),
+        (row_s_hbm, row_s),
+        (col_c_hbm, col_c),
+        (col_s_hbm, col_s),
+        (qg_hbm, qg),
+        (kg_hbm, kg),
+        (wq_hbm, wq),
+        (w_hbm, wfull.at[me]),
+    )
+    fetch = [pltpu.make_async_copy(src, dst, loc.at[i]) for i, (src, dst) in enumerate(fetches)]
+    for cp in fetch:
+        cp.start()
+    for cp in fetch[0:4]:
+        cp.wait()
 
     started = []
 
@@ -196,10 +218,6 @@
 
     def r_to(src, row, p, i, **to):
         return go(src, View(rows)[row, rpiece[p]], View(rs)[i], View(rr)[i], **to)
-
-    up = [r_to(View(lat)[rpiece[p]], me, p, p, y=yp) for p in (0, 1)]
-    down = [r_to(View(lat)[rpiece[p]], me, p, 2 + p, y=ym) for p in (1, 0)]
-    across = [go(lat, View(rows)[me], View(rs)[6], View(rr)[6], c=1 - c)]
 
     eye_in = diagonal(cond.shape[1])
     for r, ref in enumerate((cond, ctx_cond)):
@@ -207,12 +225,19 @@
         v = v * jax.nn.sigmoid(v)
         column = jnp.sum(jnp.where(eye_in, jnp.broadcast_to(v, eye_in.shape), 0.0), axis=1, keepdims=True)
         part[r : r + 1, :] = jnp.sum(column * mod_weight[...], axis=0, keepdims=True)
-    z_out = [go(part, View(zbuf)[z], View(zs)[i], View(zr)[i], **to) for i, to in enumerate(z_to)]
-    zbuf[z] = part[...]
     rows[me] = lat[...]
     acc[...] = jnp.zeros_like(acc)
     tot[...] = jnp.zeros_like(tot)
     top[...] = jnp.full_like(top, -1e30)
+    greeted()
+
+    z_out = [None] * len(z_to)
+    for i in (3, 2, 4, 1, 5, 0, 6):
+        z_out[i] = go(part, View(zbuf)[z], View(zs)[i], View(zr)[i], **z_to[i])
+    up = [r_to(View(lat)[rpiece[p]], me, p, p, y=yp) for p in (0, 1)]
+    down = [r_to(View(lat)[rpiece[p]], me, p, 2 + p, y=ym) for p in (1, 0)]
+    across = [go(lat, View(rows)[me], View(rs)[6], View(rr)[6], c=1 - c)]
+    zbuf[z] = part[...]
     got(z_out)
     px[...] = sum((zbuf[i] for i in range(1, NZ)), zbuf[0])
     x_out = [go(px, View(xbuf)[x], View(xs)[i], View(xr)[i], **to) for i, to in enumerate(x_to)]
@@ -229,7 +254,7 @@
     across.append(go(View(rows)[high], View(rows)[high], View(rs)[8], View(rr)[8], c=1 - c))
     got([up2, down2])
     across.append(go(View(rows)[far], View(rows)[far], View(rs)[9], View(rr)[9], c=1 - c))
-    for cp in fetch:
+    for cp in fetch[4:]:
         cp.wait()
 
     wh = w_hbm.shape[0] // 2
@@ -249,10 +274,12 @@
     got(across)
 
     cut = n // 2
-    kpiece = (pl.ds(0, cut), pl.ds(cut, cut + n_ctx))
+    quarter = n // 4
+    kpiece = [pl.ds(p * quarter, quarter) for p in range(3)] + [pl.ds(3 * quarter, quarter + n_ctx)]
+    plus, minus = (0, 1, 2, 3), (2, 3, 0, 1)
 
     def k_to(src, slot, p, **to):
-        i = 2 * (slot - 1) + p
+        i = 4 * (slot - 1) + p
         return go(View(kvbuf)[src, kpiece[p]], View(kvbuf)[slot, kpiece[p]], View(ks)[i], View(kr)[i], **to)
 
     def q_to(src, slot, h, **to):
@@ -276,7 +303,7 @@
         other = jnp.where(early, pltpu.roll(v, hd - hd // 4, 1), pltpu.roll(v, hd // 4, 1))
         return (v * table(row_c, col_c, i) + other * table(row_s, col_s, i)).astype(BF16)
 
-    k1, k2 = [], []
+    k1, k2 = {}, {}
     per = NTP // 2
     for i in range(2):
         for g in range(per):
@@ -290,8 +317,11 @@
             kv = jnp.dot(modulated(ctx[...], 1), wkv[...], preferred_element_type=F32)
             kvbuf[0, n : n + n_ctx, 0:hd] = (rms(kv[:, 0:hd]) * kg[...]).astype(BF16)
             kvbuf[0, n : n + n_ctx, hd : 2 * hd] = kv[:, hd : 2 * hd].astype(BF16)
-        k1.append(k_to(0, 1, i, z=zp))
-        k2.append(k_to(0, 2, i, z=zm))
+        for p in plus[2 * i : 2 * i + 2]:
+            k1[p] = k_to(0, 1, p, z=zp)
+        if i == 1:
+            for p in minus:
+                k2[p] = k_to(0, 2, p, z=zm)
     for i in range(2):
         a = normed[i * per : (i + 1) * per].reshape(cut, d)
         q = jnp.dot(a, wq[...], preferred_element_type=F32)
@@ -315,24 +345,30 @@
         tot[a, h] = tot[a, h] * factor + some
         acc[a, h] = acc[a, h] * factor + jnp.dot(p.astype(BF16), v, preferred_element_type=F32)
 
-    def tile(a, slots, tail=False):
+    def tile(works, slots, tail=False):
         more = [cbuf[...]] if tail else []
         m = n * len(slots)
         k = jnp.concatenate([kvbuf[b, 0:n, 0:hd] for b in slots] + [e[:, 0:hd] for e in more], axis=0)
         v = jnp.concatenate([kvbuf[b, 0:n, hd : 2 * hd] for b in slots] + [e[:, hd : 2 * hd] for e in more], axis=0)
-        found = [scores(a, h, k) for h in range(heads)]
-        for h in range(heads):
-            s = found[h]
+        found = [scores(a, h, k) for a, h in works]
+        for (a, h), s in zip(works, found):
             if tail:
                 s = jnp.concatenate([s[:, 0:m], s[:, m:] + raw_lift], axis=1)
             update(a, h, s, v)
 
+    def both_heads(a):
+        return [(a, h) for h in range(heads)]
+
     eye = diagonal(hd)
     blocks = n // hd
 
-    def join(a, h, others, o_to, l_to):
-        for b in range(blocks):
-            at = pl.ds(b * hd, hd)
+    parts = 2
+    pb = blocks // parts
+
+    def join(a, h, t, others, o_to, l_to):
+        for b in range(pb):
+            at = pl.ds((t * pb + b) * hd, hd)
+            here = pl.ds(b * hd, hd)
             total = jnp.sum(tot[a, h, at, :], axis=1, keepdims=True)
             value = acc[a, h, at, :] / total
             lse = top[a, h, at, :] * scale + jnp.log2(total)
@@ -342,7 +378,7 @@
                     row = jnp.broadcast_to(l_ref[b : b + 1, :], (hd, hd))
                     col = jnp.sum(jnp.where(eye, row, 0.0), axis=1, keepdims=True)
                     lses.append(jnp.broadcast_to(col, (hd, hd)))
-                    values.append(o_ref[at, :].astype(F32))
+                    values.append(o_ref[here, :].astype(F32))
                 best = functools.reduce(jnp.maximum, lses)
                 weights = [jnp.exp2(v - best) for v in lses]
                 total = sum(weights[1:], weights[0])
@@ -352,104 +388,126 @@
             if l_to is not None:
                 l_to[b : b + 1, :] = jnp.sum(jnp.where(eye, lse, 0.0), axis=0, keepdims=True)
 
-    def finish(a, h, others=()):
+    def finish(a, h, t, others=()):
         def put(b, value):
-            osend[a - 1, h, b * hd : (b + 1) * hd, :] = value
-
-        join(a, h, others, put, lsend.at[a - 1, h])
-
-    def o_go(a, h, to_o, to_l, i, **to):
-        ls = go(View(lsend)[a - 1, h], to_l, View(ls_)[i], View(lr_)[i], **to)
-        return [ls, go(View(osend)[a - 1, h], to_o, View(os_)[i], View(or_)[i], **to)]
-
-    k3, k4, k5, k6, k7, q34, w34 = [], [], [], [], [], [], []
-    got([k1[0], k2[0]])
-    k3.append(k_to(1, 3, 0, z=zp))
-    k4.append(k_to(2, 4, 0, z=zm))
-    got([k1[1], k2[1]])
-    k3.append(k_to(1, 3, 1, z=zp))
-    k4.append(k_to(2, 4, 1, z=zm))
+            osend[a - 1, h, t, b * hd : (b + 1) * hd, :] = value
+
+        join(a, h, t, others, put, lsend.at[a - 1, h, t])
+
+    def o_go(a, h, t, to_o, to_l, i, **to):
+        i = 2 * i + t
+        ls = go(View(lsend)[a - 1, h, t], to_l, View(ls_)[i], View(lr_)[i], **to)
+        return [ls, go(View(osend)[a - 1, h, t], to_o, View(os_)[i], View(or_)[i], **to)]
+
+    ring = {1: k1, 2: k2}
+    for slot in range(3, NZ):
+        ring[slot] = {}
+
+    def pass_on(hop, i):
+        src_p, src_m = 2 * hop - 1, 2 * hop
+        got([ring[src_p][plus[i]], ring[src_m][minus[i]]])
+        last = hop == 3
+        ring[src_p + 2][plus[i]] = k_to(src_p, src_p + 2, plus[i], z=zp)
+        to_slot = src_p + 2 if last else src_m + 2
+        ring[to_slot][minus[i]] = k_to(src_m, to_slot, minus[i], z=zm)
+
+    q34, w34 = [], []
+    tile(both_heads(0), (0,))
+    for i in range(4):
+        pass_on(1, i)
     got([q1[0], q2[0]])
     q34.append(q_to(1, 3, 0, x=xp))
     q34.append(q_to(2, 3, 1, x=xm))
+    tile(both_heads(0), (1, 2))
     got([q1[1], q2[1]])
 
-    def one(j, carry):
-        @pl.when(j == 1)
+    def one(a, carry):
+        @pl.when(a == 1)
         def _():
-            got([k3[0], k4[0]])
-            k5.append(k_to(3, 5, 0, z=zp))
-            k6.append(k_to(4, 6, 0, z=zm))
-
-        @pl.when(j == 3)
+            pass_on(2, 0)
+
+        @pl.when(a == 2)
         def _():
-            got([k3[1], k4[1]])
-            k5.append(k_to(3, 5, 1, z=zp))
-            k6.append(k_to(4, 6, 1, z=zm))
+            pass_on(2, 1)
+
+        @pl.when(a == 3)
+        def _():
+            pass_on(2, 2)
+            pass_on(2, 3)
             got(q34)
 
-        tile(jnp.where(j == 2, 0, jnp.where(j == 3, 3, j + 1)), (0, 1, 2))
+        tile(both_heads(a), (0, 1, 2))
         return carry
 
-    lax.fori_loop(0, 4, one, 0)
-
-    def two(j, carry):
-        @pl.when(j == 0)
+    lax.fori_loop(1, 4, one, 0)
+
+    def two(a, carry):
+        @pl.when(a == 1)
         def _():
-            got([k5[0], k6[0]])
-            k7.append(k_to(5, 7, 0, z=zp))
+            pass_on(3, 0)
+
+        @pl.when(a == 2)
+        def _():
+            pass_on(3, 1)
             got([w1[0], w2[0]])
             w34.append(w_to(low, 0, 4, y=yp))
             w34.append(w_to(high, 1, 5, y=ym))
 
-        @pl.when(j == 2)
-        def _():
-            got([k5[1], k6[1]])
-            k7.append(k_to(6, 7, 1, z=zm))
-
-        tile(jnp.where(j == 3, 0, j + 1), (3, 4))
+        tile(both_heads(a), (3, 4))
         return carry
 
-    lax.fori_loop(0, 4, two, 0)
-    got(k7)
+    lax.fori_loop(1, 4, two, 0)
+    got([ring[5][p] for p in plus[2:]] + [ring[6][p] for p in minus[2:]])
+    tile(both_heads(3), (5, 6))
+    got([ring[7][p] for p in range(4)])
     for b in range(NZ):
         cbuf[b * n_ctx : (b + 1) * n_ctx, :] = kvbuf[b, n : n + n_ctx, :]
 
     late = (5, 6, 7)
-    tile(3, late, True)
-    finish(3, 0)
-    finish(3, 1)
-    far0 = o_go(3, 0, View(orelay)[0], View(lrelay)[0], 0, x=xp)
-    far1 = o_go(3, 1, View(orelay)[1], View(lrelay)[1], 1, x=xm)
-
-    def near(a, carry):
-        tile(a, late, True)
+    tile(both_heads(3), (7,), True)
+    far0, far1, pure0, pure1, both0, both1 = [], [], [], [], [], []
+    for t in range(parts):
+        finish(3, 0, t)
+        finish(3, 1, t)
+        far0.append(o_go(3, 0, t, View(orelay)[0, t], View(lrelay)[0, t], 0, x=xp))
+        far1.append(o_go(3, 1, t, View(orelay)[1, t], View(lrelay)[1, t], 1, x=xm))
+
+    def near(i, carry):
+        tile([(1 + i, 0), (2 - i, 1)], late, True)
+
+        @pl.when(i == 0)
+        def _():
+            for t in range(parts):
+                finish(1, 0, t)
+                finish(2, 1, t)
+                pure0.append(o_go(1, 0, t, View(orecv)[1, 0, t], View(lrecv)[1, 0, t], 2, x=xm))
+                pure1.append(o_go(2, 1, t, View(orecv)[0, 1, t], View(lrecv)[0, 1, t], 3, x=xp))
+
         return carry
 
-    lax.fori_loop(1, 3, near, 0)
-    finish(1, 0)
-    finish(2, 1)
-    pure0 = o_go(1, 0, View(orecv)[1, 0], View(lrecv)[1, 0], 2, x=xm)
-    pure1 = o_go(2, 1, View(orecv)[0, 1], View(lrecv)[0, 1], 3, x=xp)
+    lax.fori_loop(0, 2, near, 0)
     got([w1[1], w2[1]])
     w5 = go(View(wfull)[low], View(wfull)[low], View(ws)[6], View(wr)[6], c=1 - c)
     w6 = go(View(wfull)[high], View(wfull)[high], View(ws)[7], View(wr)[7], c=1 - c)
-    got(far0 + far1)
-    finish(2, 0, [(orelay.at[0], lrelay.at[0])])
-    finish(1, 1, [(orelay.at[1], lrelay.at[1])])
-    both0 = o_go(2, 0, View(orecv)[0, 0], View(lrecv)[0, 0], 4, x=xp)
-    both1 = o_go(1, 1, View(orecv)[1, 1], View(lrecv)[1, 1], 5, x=xm)
-    tile(0, late, True)
+    for t in range(parts):
+        got(far0[t] + far1[t])
+        finish(2, 0, t, [(orelay.at[0, t], lrelay.at[0, t])])
+        finish(1, 1, t, [(orelay.at[1, t], lrelay.at[1, t])])
+        both0.append(o_go(2, 0, t, View(orecv)[0, 0, t], View(lrecv)[0, 0, t], 4, x=xp))
+        both1.append(o_go(1, 1, t, View(orecv)[1, 1, t], View(lrecv)[1, 1, t], 5, x=xm))
+    tile(both_heads(0), (3, 4))
+    tile(both_heads(0), late, True)
     got(w34)
     w7 = go(View(wfull)[far], View(wfull)[far], View(ws)[9], View(wr)[9], c=1 - c)
-    got(pure0 + pure1 + both0 + both1)
-
-    for h in range(heads):
-
-        def put(b, value, h=h):
-            att[b * hd : (b + 1) * hd, h * hd : (h + 1) * hd] = value
-
-        join(0, h, [(orecv.at[i, h], lrecv.at[i, h]) for i in range(2)], put, None)
+
+    for t in range(parts):
+        got(pure0[t] + pure1[t] + both0[t] + both1[t])
+        for h in range(heads):
+
+            def put(b, value, h=h, t=t):
+                att[(t * pb + b) * hd : (t * pb + b + 1) * hd, h * hd : (h + 1) * hd] = value
+
+            join(0, h, t, [(orecv.at[i, h, t], lrecv.at[i, h, t]) for i in range(2)], put, None)
 
     t_out = [None] * len(t_to)
     for i in (3, 4, 1, 2, 5, 6, 0):
@@ -504,14 +562,29 @@
     lift = math.log(tokens / (2.0 * n_ctx * NZ * NX))
     tables = [jnp.asarray(t) for t in rope_tables(tokens // GRID_W, hd)]
     dma = pltpu.SemaphoreType.DMA
-    pairs = [s for count in (10, NZ - 1, NX - 1, NTP - 1, 14, 6, 10, 6, 6, NTP - 1) for s in (dma((count,)),) * 2]
+    pairs = [s for count in (10, NZ - 1, NX - 1, NTP - 1, 28, 6, 10, 12, 12, NTP - 1) for s in (dma((count,)),) * 2]
+    inputs = (
+        latents,
+        context,
+        cond[None, :],
+        ctx_cond[None, :],
+        mod_weight,
+        query_gain[None, :],
+        key_gain[None, :],
+        *tables,
+        query_weight,
+        key_matrix,
+        value_matrix,
+        out_weight,
+    )
     return pl.pallas_call(
         functools.partial(block_kernel, lift),
         name="block_stage",
-        out_shape=jax.ShapeDtypeStruct((mine, d), BF16),
-        in_specs=[VMEM_SPEC] * 11 + [pl.BlockSpec(memory_space=pl.ANY)] * 4,
+        out_shape=pltpu.VMEM((mine, d), BF16),
+        in_specs=[pl.BlockSpec(memory_space=pl.ANY)] * len(inputs),
         out_specs=VMEM_SPEC,
-        scratch_shapes=[
+        scratch_shapes=[pltpu.VMEM(a.shape, a.dtype) for a in inputs[:11]]
+        + [
             pltpu.VMEM((NTP, mine, d), BF16),
             pltpu.VMEM((NTP, mine, d), BF16),
             pltpu.VMEM((2, NTP * cols), F32),
@@ -529,36 +602,23 @@
             pltpu.VMEM((NX, heads, n, hd), F32),
             pltpu.VMEM((NX, heads, n, hd), F32),
             pltpu.VMEM((NX, heads, n, hd), F32),
-            pltpu.VMEM((NX - 1, heads, n, hd), BF16),
-            pltpu.VMEM((NX - 1, heads, n // hd, hd), F32),
-            pltpu.VMEM((2, heads, n, hd), BF16),
-            pltpu.VMEM((2, heads, n // hd, hd), F32),
-            pltpu.VMEM((2, n, hd), BF16),
-            pltpu.VMEM((2, n // hd, hd), F32),
+            pltpu.VMEM((NX - 1, heads, 2, n // 2, hd), BF16),
+            pltpu.VMEM((NX - 1, heads, 2, n // hd // 2, hd), F32),
+            pltpu.VMEM((2, heads, 2, n // 2, hd), BF16),
+            pltpu.VMEM((2, heads, 2, n // hd // 2, hd), F32),
+            pltpu.VMEM((2, 2, n // 2, hd), BF16),
+            pltpu.VMEM((2, 2, n // hd // 2, hd), F32),
             pltpu.VMEM((NTP,) + out_weight.shape, BF16),
             pltpu.VMEM((n, heads * hd), BF16),
             pltpu.VMEM((NTP, mine, heads * hd), BF16),
             pltpu.VMEM((mine, d), F32),
-            dma((4,)),
+            dma((15,)),
         ]
         + pairs,
         compiler_params=pltpu.CompilerParams(
             collective_id=0, has_side_effects=True, vmem_limit_bytes=62 * 1024 * 1024
         ),
-    )(
-        latents,
-        context,
-        cond[None, :],
-        ctx_cond[None, :],
-        mod_weight,
-        query_gain[None, :],
-        key_gain[None, :],
-        *tables,
-        query_weight,
-        key_matrix,
-        value_matrix,
-        out_weight,
-    )
+    )(*inputs)
 
 
 def solution(mesh):

time: 77.7 us -> 69.9 us (0.90)
  Pallas kernels: 75.8 us -> 69.2 us
  local copies, waits for them, and re-layouts: 1.67 us -> 0.71 us
    pallas_call x1, Pallas kernels: 75.8 us -> 69.2 us  [body(): pl.pallas_call(functools.partial(block_kernel, lift), name='block_stage',...]
    unnamed x1, local copies, waits for them, and re-layouts: 1.67 us -> 0.71 us
where the time goes in v3:
time: 69.9 us
  Pallas kernels  69.2 us (99%)
  local copies, waits for them, and re-layouts  0.71 us (1%)
    pallas_call x1, Pallas kernels, body(): pl.pallas_call(functools.partial(block_kernel, lift), name='block_stage',...  69.2 us

profile of v3, /device:TPU:1, one launch (start us, length us, event | category | flops | bytes accessed | tf_op | source)
XLA Modules:
  0.0 69.9 jit_solution(14020318479905432243)
XLA Ops:
  0.0 69.2 %block_stage.1 = bf16[64,2048]{1,0:T(8,128)(2,1)S(1)} custom-call(bf16[64,2048]{1,0:T(8,128)(2,1)} %refs_0_.1, bf16[16,2048]{1,0:T(8,128)(2,1)} %refs_1_.1, f32[1,64]{1,0:T(1,128)} %bitcast.4, f32[1,64]{1,0:T(1,128)} %bitcast.5, f32[64,768]{1,0:T(8,128)} %refs_4_.1, f32[1,128]{1,0:T(1,128)} %bitcast.6, f32[1,128]{1,0:T(1,128)} %bitcast.7, ...), custom_call_target="tpu_custom_call" | custom-call | tf_op jit(solution)/shard_map/block_stage/pallas_call | solution.py:580
  69.2 0.7 %copy.17 = bf16[64,2048]{1,0:T(8,128)(2,1)} copy(bf16[64,2048]{1,0:T(8,128)(2,1)S(1)} %block_stage.1) | data formatting | bytes 524288

commit v4 on v3

--- a/solution.py
+++ b/solution.py
@@ -201,23 +201,24 @@
     for cp in fetch[0:4]:
         cp.wait()
 
-    started = []
-
-    def go(*args, **to):
-        cp = functools.partial(make, *args, **to)
-        cp().start()
-        started.append(cp)
-        return cp
-
-    def got(copies):
-        for cp in copies:
-            cp().wait_recv()
+    def go(src, dst, sems, i, **to):
+        make(src, dst, View(sems[0])[0], View(sems[1])[i], **to).start()
+
+    def got(view, sems, i):
+        make(view, view, View(sems[0])[0], View(sems[1])[i], c=1 - c).wait_recv()
+
+    def gone(view, sems):
+        make(view, view, View(sems[0])[0], View(sems[1])[0], c=1 - c).wait_send()
+
+    r_, z_, x_, m_, k_, q_, w_, o_, l_, t_ = (
+        (rs, rr), (zs, zr), (xs, xr), (ms, mr), (ks, kr), (qs, qr), (ws, wr), (os_, or_), (ls_, lr_), (ts, tr),
+    )
 
     rh = mine // 2
     rpiece = (pl.ds(0, rh), pl.ds(rh, rh))
 
     def r_to(src, row, p, i, **to):
-        return go(src, View(rows)[row, rpiece[p]], View(rs)[i], View(rr)[i], **to)
+        go(src, View(rows)[row, rpiece[p]], r_, i, **to)
 
     eye_in = diagonal(cond.shape[1])
     for r, ref in enumerate((cond, ctx_cond)):
@@ -231,29 +232,31 @@
     top[...] = jnp.full_like(top, -1e30)
     greeted()
 
-    z_out = [None] * len(z_to)
     for i in (3, 2, 4, 1, 5, 0, 6):
-        z_out[i] = go(part, View(zbuf)[z], View(zs)[i], View(zr)[i], **z_to[i])
-    up = [r_to(View(lat)[rpiece[p]], me, p, p, y=yp) for p in (0, 1)]
-    down = [r_to(View(lat)[rpiece[p]], me, p, 2 + p, y=ym) for p in (1, 0)]
-    across = [go(lat, View(rows)[me], View(rs)[6], View(rr)[6], c=1 - c)]
+        go(part, View(zbuf)[z], z_, 0, **z_to[i])
+    for i in range(2):
+        r_to(View(lat)[rpiece[i]], me, i, i, y=yp)
+        r_to(View(lat)[rpiece[1 - i]], me, 1 - i, i, y=ym)
+    go(lat, View(rows)[me], r_, 3, c=1 - c)
     zbuf[z] = part[...]
-    got(z_out)
+    got(View(zbuf)[0 : NZ - 1], z_, 0)
     px[...] = sum((zbuf[i] for i in range(1, NZ)), zbuf[0])
-    x_out = [go(px, View(xbuf)[x], View(xs)[i], View(xr)[i], **to) for i, to in enumerate(x_to)]
+    for to in x_to:
+        go(px, View(xbuf)[x], x_, 0, **to)
     xbuf[x] = px[...]
-    got([up[0], down[0]])
-    up2 = r_to(View(rows)[low, rpiece[0]], low, 0, 4, y=yp)
-    down2 = r_to(View(rows)[high, rpiece[1]], high, 1, 5, y=ym)
-    got(x_out)
+    got(View(rows)[0], r_, 0)
+    r_to(View(rows)[low, rpiece[0]], low, 0, 2, y=yp)
+    r_to(View(rows)[high, rpiece[1]], high, 1, 2, y=ym)
+    got(View(xbuf)[0 : NX - 1], x_, 0)
     pt[...] = sum((xbuf[i] for i in range(1, NX)), xbuf[0])
-    m_out = [go(pt, View(tbuf)[me], View(ms)[i], View(mr)[i], **to) for i, to in enumerate(t_to)]
+    for to in t_to:
+        go(pt, View(tbuf)[me], m_, 0, **to)
     tbuf[me] = pt[...]
-    got([up[1], down[1]])
-    across.append(go(View(rows)[low], View(rows)[low], View(rs)[7], View(rr)[7], c=1 - c))
-    across.append(go(View(rows)[high], View(rows)[high], View(rs)[8], View(rr)[8], c=1 - c))
-    got([up2, down2])
-    across.append(go(View(rows)[far], View(rows)[far], View(rs)[9], View(rr)[9], c=1 - c))
+    got(View(rows)[0], r_, 1)
+    go(View(rows)[low], View(rows)[low], r_, 3, c=1 - c)
+    go(View(rows)[high], View(rows)[high], r_, 3, c=1 - c)
+    got(View(rows)[0], r_, 2)
+    go(View(rows)[far], View(rows)[far], r_, 3, c=1 - c)
     for cp in fetch[4:]:
         cp.wait()
 
@@ -262,16 +265,17 @@
 
     def w_to(row, p, i, **to):
         piece = View(wfull)[row, wpiece[p]]
-        return go(piece, piece, View(ws)[i], View(wr)[i], **to)
-
-    w1 = [w_to(me, p, p, y=yp) for p in (0, 1)]
-    w2 = [w_to(me, p, 2 + p, y=ym) for p in (1, 0)]
-    w0 = go(View(wfull)[me], View(wfull)[me], View(ws)[8], View(wr)[8], c=1 - c)
-    got(m_out)
+        go(piece, piece, w_, i, **to)
+
+    for i in range(2):
+        w_to(me, i, i, y=yp)
+        w_to(me, 1 - i, i, y=ym)
+    go(View(wfull)[me], View(wfull)[me], w_, 3, c=1 - c)
+    got(View(tbuf)[0 : NTP - 1], m_, 0)
     w = part.shape[1]
     for i in range(NTP):
         mod[:, i * w : (i + 1) * w] = tbuf[i]
-    got(across)
+    got(View(rows)[0:4], r_, 3)
 
     cut = n // 2
     quarter = n // 4
@@ -279,12 +283,16 @@
     plus, minus = (0, 1, 2, 3), (2, 3, 0, 1)
 
     def k_to(src, slot, p, **to):
-        i = 4 * (slot - 1) + p
-        return go(View(kvbuf)[src, kpiece[p]], View(kvbuf)[slot, kpiece[p]], View(ks)[i], View(kr)[i], **to)
-
-    def q_to(src, slot, h, **to):
-        i = 2 * (slot - 1) + h
-        return go(View(qbuf)[src, h], View(qbuf)[slot, h], View(qs)[i], View(qr)[i], **to)
+        order = plus if slot % 2 else minus
+        i = 12 if slot == NZ - 1 else 4 * ((slot - 1) // 2) + order.index(p)
+        go(View(kvbuf)[src, kpiece[p]], View(kvbuf)[slot, kpiece[p]], k_, i, **to)
+
+    def k_got(hop, i):
+        count = kpiece[plus[i]].size + kpiece[minus[i]].size
+        got(View(kvbuf)[0, 0:count], k_, 4 * (hop - 1) + i)
+
+    def q_to(src, slot, h, i, **to):
+        go(View(qbuf)[src, h], View(qbuf)[slot, h], q_, i, **to)
 
     def modulated(v, r):
         v = rms(v.astype(F32))
@@ -303,7 +311,6 @@
         other = jnp.where(early, pltpu.roll(v, hd - hd // 4, 1), pltpu.roll(v, hd // 4, 1))
         return (v * table(row_c, col_c, i) + other * table(row_s, col_s, i)).astype(BF16)
 
-    k1, k2 = {}, {}
     per = NTP // 2
     for i in range(2):
         for g in range(per):
@@ -318,18 +325,19 @@
             kvbuf[0, n : n + n_ctx, 0:hd] = (rms(kv[:, 0:hd]) * kg[...]).astype(BF16)
             kvbuf[0, n : n + n_ctx, hd : 2 * hd] = kv[:, hd : 2 * hd].astype(BF16)
         for p in plus[2 * i : 2 * i + 2]:
-            k1[p] = k_to(0, 1, p, z=zp)
+            k_to(0, 1, p, z=zp)
         if i == 1:
             for p in minus:
-                k2[p] = k_to(0, 2, p, z=zm)
+                k_to(0, 2, p, z=zm)
     for i in range(2):
         a = normed[i * per : (i + 1) * per].reshape(cut, d)
         q = jnp.dot(a, wq[...], preferred_element_type=F32)
         for h in range(heads):
             at = slice(i * cut, (i + 1) * cut)
             qbuf[0, h, at, :] = turned(rms(q[:, h * hd : (h + 1) * hd]) * qg[...], i)
-    q1 = [q_to(0, 1, h, x=xp) for h in (0, 1)]
-    q2 = [q_to(0, 2, h, x=xm) for h in (1, 0)]
+    for i in range(2):
+        q_to(0, 1, i, i, x=xp)
+        q_to(0, 2, 1 - i, i, x=xm)
 
     def scores(a, h, k):
         return lax.dot_general(qbuf[a, h], k, (((1,), (1,)), ((), ())), preferred_element_type=F32)
@@ -346,10 +354,14 @@
         acc[a, h] = acc[a, h] * factor + jnp.dot(p.astype(BF16), v, preferred_element_type=F32)
 
     def tile(works, slots, tail=False):
-        more = [cbuf[...]] if tail else []
-        m = n * len(slots)
-        k = jnp.concatenate([kvbuf[b, 0:n, 0:hd] for b in slots] + [e[:, 0:hd] for e in more], axis=0)
-        v = jnp.concatenate([kvbuf[b, 0:n, hd : 2 * hd] for b in slots] + [e[:, hd : 2 * hd] for e in more], axis=0)
+        spans = [b if isinstance(b, tuple) else (b, 0, n) for b in slots]
+        m = sum(hi - lo for _, lo, hi in spans)
+
+        def take(lane):
+            at = slice(lane, lane + hd)
+            return jnp.concatenate([kvbuf[b, lo:hi, at] for b, lo, hi in spans] + ([cbuf[:, at]] if tail else []), axis=0)
+
+        k, v = take(0), take(hd)
         found = [scores(a, h, k) for a, h in works]
         for (a, h), s in zip(works, found):
             if tail:
@@ -395,31 +407,30 @@
         join(a, h, t, others, put, lsend.at[a - 1, h, t])
 
     def o_go(a, h, t, to_o, to_l, i, **to):
-        i = 2 * i + t
-        ls = go(View(lsend)[a - 1, h, t], to_l, View(ls_)[i], View(lr_)[i], **to)
-        return [ls, go(View(osend)[a - 1, h, t], to_o, View(os_)[i], View(or_)[i], **to)]
-
-    ring = {1: k1, 2: k2}
-    for slot in range(3, NZ):
-        ring[slot] = {}
+        go(View(lsend)[a - 1, h, t], to_l, l_, i, **to)
+        go(View(osend)[a - 1, h, t], to_o, o_, i, **to)
+
+    def o_got(o_view, l_view, i):
+        got(l_view, l_, i)
+        got(o_view, o_, i)
 
     def pass_on(hop, i):
         src_p, src_m = 2 * hop - 1, 2 * hop
-        got([ring[src_p][plus[i]], ring[src_m][minus[i]]])
-        last = hop == 3
-        ring[src_p + 2][plus[i]] = k_to(src_p, src_p + 2, plus[i], z=zp)
-        to_slot = src_p + 2 if last else src_m + 2
-        ring[to_slot][minus[i]] = k_to(src_m, to_slot, minus[i], z=zm)
-
-    q34, w34 = [], []
+        k_got(hop, i)
+        k_to(src_p, src_p + 2, plus[i], z=zp)
+        k_to(src_m, src_p + 2 if hop == 3 else src_m + 2, minus[i], z=zm)
+
     tile(both_heads(0), (0,))
-    for i in range(4):
-        pass_on(1, i)
-    got([q1[0], q2[0]])
-    q34.append(q_to(1, 3, 0, x=xp))
-    q34.append(q_to(2, 3, 1, x=xm))
-    tile(both_heads(0), (1, 2))
-    got([q1[1], q2[1]])
+    pass_on(1, 0)
+    pass_on(1, 1)
+    tile(both_heads(0), ((1, 0, cut), (2, cut, n)))
+    pass_on(1, 2)
+    pass_on(1, 3)
+    got(View(qbuf)[1], q_, 0)
+    q_to(1, 3, 0, 2, x=xp)
+    q_to(2, 3, 1, 2, x=xm)
+    tile(both_heads(0), ((1, cut, n), (2, 0, cut)))
+    got(View(qbuf)[1], q_, 1)
 
     def one(a, carry):
         @pl.when(a == 1)
@@ -434,7 +445,7 @@
         def _():
             pass_on(2, 2)
             pass_on(2, 3)
-            got(q34)
+            got(View(qbuf)[1], q_, 2)
 
         tile(both_heads(a), (0, 1, 2))
         return carry
@@ -449,28 +460,28 @@
         @pl.when(a == 2)
         def _():
             pass_on(3, 1)
-            got([w1[0], w2[0]])
-            w34.append(w_to(low, 0, 4, y=yp))
-            w34.append(w_to(high, 1, 5, y=ym))
+            got(View(wfull)[0], w_, 0)
+            w_to(low, 0, 2, y=yp)
+            w_to(high, 1, 2, y=ym)
 
         tile(both_heads(a), (3, 4))
         return carry
 
     lax.fori_loop(1, 4, two, 0)
-    got([ring[5][p] for p in plus[2:]] + [ring[6][p] for p in minus[2:]])
+    k_got(3, 2)
+    k_got(3, 3)
     tile(both_heads(3), (5, 6))
-    got([ring[7][p] for p in range(4)])
+    got(View(kvbuf)[0], k_, 12)
     for b in range(NZ):
         cbuf[b * n_ctx : (b + 1) * n_ctx, :] = kvbuf[b, n : n + n_ctx, :]
 
     late = (5, 6, 7)
     tile(both_heads(3), (7,), True)
-    far0, far1, pure0, pure1, both0, both1 = [], [], [], [], [], []
     for t in range(parts):
         finish(3, 0, t)
         finish(3, 1, t)
-        far0.append(o_go(3, 0, t, View(orelay)[0, t], View(lrelay)[0, t], 0, x=xp))
-        far1.append(o_go(3, 1, t, View(orelay)[1, t], View(lrelay)[1, t], 1, x=xm))
+        o_go(3, 0, t, View(orelay)[0, t], View(lrelay)[0, t], t, x=xp)
+        o_go(3, 1, t, View(orelay)[1, t], View(lrelay)[1, t], t, x=xm)
 
     def near(i, carry):
         tile([(1 + i, 0), (2 - i, 1)], late, True)
@@ -480,28 +491,28 @@
             for t in range(parts):
                 finish(1, 0, t)
                 finish(2, 1, t)
-                pure0.append(o_go(1, 0, t, View(orecv)[1, 0, t], View(lrecv)[1, 0, t], 2, x=xm))
-                pure1.append(o_go(2, 1, t, View(orecv)[0, 1, t], View(lrecv)[0, 1, t], 3, x=xp))
+                o_go(1, 0, t, View(orecv)[1, 0, t], View(lrecv)[1, 0, t], parts + t, x=xm)
+                o_go(2, 1, t, View(orecv)[0, 1, t], View(lrecv)[0, 1, t], parts + t, x=xp)
 
         return carry
 
     lax.fori_loop(0, 2, near, 0)
-    got([w1[1], w2[1]])
-    w5 = go(View(wfull)[low], View(wfull)[low], View(ws)[6], View(wr)[6], c=1 - c)
-    w6 = go(View(wfull)[high], View(wfull)[high], View(ws)[7], View(wr)[7], c=1 - c)
+    got(View(wfull)[0], w_, 1)
+    go(View(wfull)[low], View(wfull)[low], w_, 4, c=1 - c)
+    go(View(wfull)[high], View(wfull)[high], w_, 4, c=1 - c)
     for t in range(parts):
-        got(far0[t] + far1[t])
+        o_got(View(orelay)[0], View(lrelay)[0], t)
         finish(2, 0, t, [(orelay.at[0, t], lrelay.at[0, t])])
         finish(1, 1, t, [(orelay.at[1, t], lrelay.at[1, t])])
-        both0.append(o_go(2, 0, t, View(orecv)[0, 0, t], View(lrecv)[0, 0, t], 4, x=xp))
-        both1.append(o_go(1, 1, t, View(orecv)[1, 1, t], View(lrecv)[1, 1, t], 5, x=xm))
+        o_go(2, 0, t, View(orecv)[0, 0, t], View(lrecv)[0, 0, t], parts + t, x=xp)
+        o_go(1, 1, t, View(orecv)[1, 1, t], View(lrecv)[1, 1, t], parts + t, x=xm)
     tile(both_heads(0), (3, 4))
     tile(both_heads(0), late, True)
-    got(w34)
-    w7 = go(View(wfull)[far], View(wfull)[far], View(ws)[9], View(wr)[9], c=1 - c)
+    got(View(wfull)[0], w_, 2)
+    go(View(wfull)[far], View(wfull)[far], w_, 5, c=1 - c)
 
     for t in range(parts):
-        got(pure0[t] + pure1[t] + both0[t] + both1[t])
+        o_got(View(orecv)[0], View(lrecv)[0], parts + t)
         for h in range(heads):
 
             def put(b, value, h=h, t=t):
@@ -509,10 +520,9 @@
 
             join(0, h, t, [(orecv.at[i, h, t], lrecv.at[i, h, t]) for i in range(2)], put, None)
 
-    t_out = [None] * len(t_to)
     for i in (3, 4, 1, 2, 5, 6, 0):
         at = pl.multiple_of(tp_index(t_to[i], y, c) * mine, mine)
-        t_out[i] = go(View(att)[pl.ds(at, mine), :], View(exch)[me], View(ts)[i], View(tr)[i], **t_to[i])
+        go(View(att)[pl.ds(at, mine), :], View(exch)[me], t_, i, **t_to[i])
     exch[me] = att[pl.ds(pl.multiple_of(me * mine, mine), mine), :]
 
     def add(source, fresh=False):
@@ -520,22 +530,34 @@
         mixed[...] = product if fresh else mixed[...] + product
 
     def came(i):
-        got([t_out[i]])
+        got(View(exch)[0], t_, i)
         back = {1: 5, 2: 6, 5: 1, 6: 2}.get(i, i)
         add(tp_index(t_to[back], y, c))
 
     add(me, True)
-    got([w0])
+    got(View(wfull)[0], w_, 3)
     came(0)
-    got([w5, w6])
+    got(View(wfull)[0:2], w_, 4)
     for i in (1, 2, 5, 6):
         came(i)
-    got([w7])
+    got(View(wfull)[0], w_, 5)
     for i in (3, 4):
         came(i)
     out[...] = (lat[...].astype(F32) + mod[0:1, 2 * d : 3 * d] * rms(mixed[...])).astype(BF16)
-    for cp in started:
-        cp().wait_send()
+    sent = (
+        (View(rows)[0 : NTP - 1], r_),
+        (View(zbuf)[0 : NZ - 1], z_),
+        (View(xbuf)[0 : NX - 1], x_),
+        (View(tbuf)[0 : NTP - 1], m_),
+        (View(kvbuf)[1:NZ], k_),
+        (View(qbuf)[1:NX], q_),
+        (View(wfull)[0 : NTP - 1], w_),
+        (osend, o_),
+        (lsend, l_),
+        (View(exch)[0 : NTP - 1], t_),
+    )
+    for view, sems in sent:
+        gone(view, sems)
 
 
 def body(
@@ -562,7 +584,8 @@
     lift = math.log(tokens / (2.0 * n_ctx * NZ * NX))
     tables = [jnp.asarray(t) for t in rope_tables(tokens // GRID_W, hd)]
     dma = pltpu.SemaphoreType.DMA
-    pairs = [s for count in (10, NZ - 1, NX - 1, NTP - 1, 28, 6, 10, 12, 12, NTP - 1) for s in (dma((count,)),) * 2]
+    kinds = (4, 1, 1, 1, 13, 3, 6, 4, 4, NTP - 1)
+    pairs = [dma((c,)) for count in kinds for c in (1, count)]
     inputs = (
         latents,
         context,

time: 69.9 us -> 68.2 us (0.976)
  Pallas kernels: 69.2 us -> 67.5 us
    pallas_call x1, Pallas kernels: 69.2 us -> 67.5 us  [body(): pl.pallas_call(functools.partial(block_kernel, lift), name='block_stage',...]
where the time goes in v4:
time: 68.2 us
  Pallas kernels  67.5 us (99%)
  local copies, waits for them, and re-layouts  0.71 us (1%)
    pallas_call x1, Pallas kernels, body(): pl.pallas_call(functools.partial(block_kernel, lift), name='block_stage',...  67.5 us

profile of v4, /device:TPU:1, one launch (start us, length us, event | category | flops | bytes accessed | tf_op | source)
XLA Modules:
  0.0 68.2 jit_solution(1390225261347155122)
XLA Ops:
  0.0 67.5 %block_stage.1 = bf16[64,2048]{1,0:T(8,128)(2,1)S(1)} custom-call(bf16[64,2048]{1,0:T(8,128)(2,1)} %refs_0_.1, bf16[16,2048]{1,0:T(8,128)(2,1)} %refs_1_.1, f32[1,64]{1,0:T(1,128)} %bitcast.4, f32[1,64]{1,0:T(1,128)} %bitcast.5, f32[64,768]{1,0:T(8,128)} %refs_4_.1, f32[1,128]{1,0:T(1,128)} %bitcast.6, f32[1,128]{1,0:T(1,128)} %bitcast.7, ...), custom_call_target="tpu_custom_call" | custom-call | tf_op jit(solution)/shard_map/block_stage/pallas_call | solution.py:603
  67.5 0.7 %copy.17 = bf16[64,2048]{1,0:T(8,128)(2,1)} copy(bf16[64,2048]{1,0:T(8,128)(2,1)S(1)} %block_stage.1) | data formatting | bytes 524288

commit v5 on v4

--- a/solution.py
+++ b/solution.py
@@ -329,12 +329,15 @@
         if i == 1:
             for p in minus:
                 k_to(0, 2, p, z=zm)
-    for i in range(2):
-        a = normed[i * per : (i + 1) * per].reshape(cut, d)
+    def queries(i, carry):
+        a = normed[pl.ds(i * per, per)].reshape(cut, d)
         q = jnp.dot(a, wq[...], preferred_element_type=F32)
+        at = pl.ds(pl.multiple_of(i * cut, cut), cut)
         for h in range(heads):
-            at = slice(i * cut, (i + 1) * cut)
             qbuf[0, h, at, :] = turned(rms(q[:, h * hd : (h + 1) * hd]) * qg[...], i)
+        return carry
+
+    lax.fori_loop(0, 2, queries, 0)
     for i in range(2):
         q_to(0, 1, i, i, x=xp)
         q_to(0, 2, 1 - i, i, x=xm)
@@ -432,42 +435,22 @@
     tile(both_heads(0), ((1, cut, n), (2, 0, cut)))
     got(View(qbuf)[1], q_, 1)
 
-    def one(a, carry):
-        @pl.when(a == 1)
-        def _():
-            pass_on(2, 0)
-
-        @pl.when(a == 2)
-        def _():
-            pass_on(2, 1)
-
-        @pl.when(a == 3)
-        def _():
+    for a in range(1, 4):
+        if a < 3:
+            pass_on(2, a - 1)
+        else:
             pass_on(2, 2)
             pass_on(2, 3)
             got(View(qbuf)[1], q_, 2)
-
         tile(both_heads(a), (0, 1, 2))
-        return carry
-
-    lax.fori_loop(1, 4, one, 0)
-
-    def two(a, carry):
-        @pl.when(a == 1)
-        def _():
-            pass_on(3, 0)
-
-        @pl.when(a == 2)
-        def _():
-            pass_on(3, 1)
+    for a in range(1, 4):
+        if a < 3:
+            pass_on(3, a - 1)
+        if a == 2:
             got(View(wfull)[0], w_, 0)
             w_to(low, 0, 2, y=yp)
             w_to(high, 1, 2, y=ym)
-
         tile(both_heads(a), (3, 4))
-        return carry
-
-    lax.fori_loop(1, 4, two, 0)
     k_got(3, 2)
     k_got(3, 3)
     tile(both_heads(3), (5, 6))
@@ -483,20 +466,13 @@
         o_go(3, 0, t, View(orelay)[0, t], View(lrelay)[0, t], t, x=xp)
         o_go(3, 1, t, View(orelay)[1, t], View(lrelay)[1, t], t, x=xm)
 
-    def near(i, carry):
-        tile([(1 + i, 0), (2 - i, 1)], late, True)
-
-        @pl.when(i == 0)
-        def _():
-            for t in range(parts):
-                finish(1, 0, t)
-                finish(2, 1, t)
-                o_go(1, 0, t, View(orecv)[1, 0, t], View(lrecv)[1, 0, t], parts + t, x=xm)
-                o_go(2, 1, t, View(orecv)[0, 1, t], View(lrecv)[0, 1, t], parts + t, x=xp)
-
-        return carry
-
-    lax.fori_loop(0, 2, near, 0)
+    tile([(1, 0), (2, 1)], late, True)
+    for t in range(parts):
+        finish(1, 0, t)
+        finish(2, 1, t)
+        o_go(1, 0, t, View(orecv)[1, 0, t], View(lrecv)[1, 0, t], parts + t, x=xm)
+        o_go(2, 1, t, View(orecv)[0, 1, t], View(lrecv)[0, 1, t], parts + t, x=xp)
+    tile([(2, 0), (1, 1)], late, True)
     got(View(wfull)[0], w_, 1)
     go(View(wfull)[low], View(wfull)[low], w_, 4, c=1 - c)
     go(View(wfull)[high], View(wfull)[high], w_, 4, c=1 - c)

time: 68.2 us -> 66.7 us (0.978)
  Pallas kernels: 67.5 us -> 65.9 us
    pallas_call x1, Pallas kernels: 67.5 us -> 65.9 us  [body(): pl.pallas_call(functools.partial(block_kernel, lift), name='block_stage',...]
where the time goes in v5:
time: 66.7 us
  Pallas kernels  65.9 us (99%)
  local copies, waits for them, and re-layouts  0.71 us (1%)
    pallas_call x1, Pallas kernels, body(): pl.pallas_call(functools.partial(block_kernel, lift), name='block_stage',...  65.9 us

profile of v5, /device:TPU:1, one launch (start us, length us, event | category | flops | bytes accessed | tf_op | source)
XLA Modules:
  0.0 66.7 jit_solution(450141704694075834)
XLA Ops:
  0.0 65.9 %block_stage.1 = bf16[64,2048]{1,0:T(8,128)(2,1)S(1)} custom-call(bf16[64,2048]{1,0:T(8,128)(2,1)} %refs_0_.1, bf16[16,2048]{1,0:T(8,128)(2,1)} %refs_1_.1, f32[1,64]{1,0:T(1,128)} %bitcast.4, f32[1,64]{1,0:T(1,128)} %bitcast.5, f32[64,768]{1,0:T(8,128)} %refs_4_.1, f32[1,128]{1,0:T(1,128)} %bitcast.6, f32[1,128]{1,0:T(1,128)} %bitcast.7, ...), custom_call_target="tpu_custom_call" | custom-call | tf_op jit(solution)/shard_map/block_stage/pallas_call | solution.py:579
  65.9 0.7 %copy.17 = bf16[64,2048]{1,0:T(8,128)(2,1)} copy(bf16[64,2048]{1,0:T(8,128)(2,1)S(1)} %block_stage.1) | data formatting | bytes 524288

commit v6 on v5

--- a/solution.py
+++ b/solution.py
@@ -298,43 +298,44 @@
         v = rms(v.astype(F32))
         return (v * (1.0 + mod[r : r + 1, d : 2 * d]) + mod[r : r + 1, 0:d]).astype(BF16)
 
-    groups = cut // GRID_W
     first = (z * NX + x) * (n // GRID_W)
-    lane = lax.broadcasted_iota(jnp.int32, (cut, hd), 1)
-    early = lax.rem(lane, hd // 2) < hd // 4
-
-    def table(row_table, col_table, i):
-        at = [first + i * groups + g for g in range(groups)]
+
+    def table(row_table, col_table, begin, count):
+        at = [first + begin + g for g in range(count)]
         return jnp.concatenate([row_table[pl.ds(t, 1), :] + col_table[...] for t in at], axis=0)
 
-    def turned(v, i):
+    def turned(v, begin):
+        count = v.shape[0] // GRID_W
+        lane = lax.broadcasted_iota(jnp.int32, v.shape, 1)
+        early = lax.rem(lane, hd // 2) < hd // 4
         other = jnp.where(early, pltpu.roll(v, hd - hd // 4, 1), pltpu.roll(v, hd // 4, 1))
-        return (v * table(row_c, col_c, i) + other * table(row_s, col_s, i)).astype(BF16)
-
-    per = NTP // 2
-    for i in range(2):
+        cos, sin = table(row_c, col_c, begin, count), table(row_s, col_s, begin, count)
+        return (v * cos + other * sin).astype(BF16)
+
+    per = NTP // 4
+    for i in (0, 2, 1, 3):
         for g in range(per):
             normed[i * per + g] = modulated(rows[i * per + g], 0)
-        a = normed[i * per : (i + 1) * per].reshape(cut, d)
+        a = normed[i * per : (i + 1) * per].reshape(quarter, d)
         kv = jnp.dot(a, wkv[...], preferred_element_type=F32)
-        at = slice(i * cut, (i + 1) * cut)
-        kvbuf[0, at, 0:hd] = turned(rms(kv[:, 0:hd]) * kg[...], i)
+        at = slice(i * quarter, (i + 1) * quarter)
+        kvbuf[0, at, 0:hd] = turned(rms(kv[:, 0:hd]) * kg[...], i * (quarter // GRID_W))
         kvbuf[0, at, hd : 2 * hd] = kv[:, hd : 2 * hd].astype(BF16)
-        if i == 1:
+        if i == 3:
             kv = jnp.dot(modulated(ctx[...], 1), wkv[...], preferred_element_type=F32)
             kvbuf[0, n : n + n_ctx, 0:hd] = (rms(kv[:, 0:hd]) * kg[...]).astype(BF16)
             kvbuf[0, n : n + n_ctx, hd : 2 * hd] = kv[:, hd : 2 * hd].astype(BF16)
-        for p in plus[2 * i : 2 * i + 2]:
+        for p in {0: (0,), 1: (1, 2), 2: (), 3: (3,)}[i]:
             k_to(0, 1, p, z=zp)
-        if i == 1:
-            for p in minus:
-                k_to(0, 2, p, z=zm)
+        for p in {0: (), 1: (), 2: (2,), 3: (3, 0, 1)}[i]:
+            k_to(0, 2, p, z=zm)
+
     def queries(i, carry):
-        a = normed[pl.ds(i * per, per)].reshape(cut, d)
+        a = normed[pl.ds(i * 2 * per, 2 * per)].reshape(cut, d)
         q = jnp.dot(a, wq[...], preferred_element_type=F32)
         at = pl.ds(pl.multiple_of(i * cut, cut), cut)
         for h in range(heads):
-            qbuf[0, h, at, :] = turned(rms(q[:, h * hd : (h + 1) * hd]) * qg[...], i)
+            qbuf[0, h, at, :] = turned(rms(q[:, h * hd : (h + 1) * hd]) * qg[...], i * (cut // GRID_W))
         return carry
 
     lax.fori_loop(0, 2, queries, 0)

time: 66.7 us -> 66.9 us (level)
  no operation moved by 1% of the time
where the time goes in v6:
time: 66.9 us; the launch traced here: 66.8 us
  Pallas kernels  66.1 us (99%)
  local copies, waits for them, and re-layouts  0.71 us (1%)
    pallas_call x1, Pallas kernels, body(): pl.pallas_call(functools.partial(block_kernel, lift), name='block_stage',...  66.1 us

profile of v6, /device:TPU:1, one launch (start us, length us, event | category | flops | bytes accessed | tf_op | source)
XLA Modules:
  0.0 66.8 jit_solution(14148347733782628634)
XLA Ops:
  0.0 66.1 %block_stage.1 = bf16[64,2048]{1,0:T(8,128)(2,1)S(1)} custom-call(bf16[64,2048]{1,0:T(8,128)(2,1)} %refs_0_.1, bf16[16,2048]{1,0:T(8,128)(2,1)} %refs_1_.1, f32[1,64]{1,0:T(1,128)} %bitcast.4, f32[1,64]{1,0:T(1,128)} %bitcast.5, f32[64,768]{1,0:T(8,128)} %refs_4_.1, f32[1,128]{1,0:T(1,128)} %bitcast.6, f32[1,128]{1,0:T(1,128)} %bitcast.7, ...), custom_call_target="tpu_custom_call" | custom-call | tf_op jit(solution)/shard_map/block_stage/pallas_call | solution.py:580
  66.1 0.7 %copy.17 = bf16[64,2048]{1,0:T(8,128)(2,1)} copy(bf16[64,2048]{1,0:T(8,128)(2,1)S(1)} %block_stage.1) | data formatting | bytes 524288
